TPU v7x, 32 devices: a whole 2x2x4 slice. The times are simulated.
32 devices in a mesh: grp: 2 (over x), ep: 8 (over z, y), tp: 2 (over core).
Axes of the slice: x: 2, y: 2, z: 4, core: 2. Of those that a mesh axis runs over, the one named last changes fastest.
Arguments:
- tokens: bfloat16 [8192, 2048], P(('grp', 'ep'), 'tp'), parts along dimension 0, may hold values from -6 to 6
- norm_gain: float32 [2048], replicated, may hold values from 0.1 to 1.9
- expert_ids: int32 [8192, 2], P(('grp', 'ep')), parts along dimension 0, may hold values from 0 to 7, all different within a row; in each aligned block of 512 rows (0 to 511, 512 to 1023, ...) at most 192 rows name the same one
- route_weights: float32 [8192, 2], P(('grp', 'ep')), parts along dimension 0, may hold values from 0.1 to 1
- gate_weight: bfloat16 [8, 2048, 512], P('ep', None, 'tp'), may hold values from -0.125 to 0.125
- up_weight: bfloat16 [8, 2048, 512], P('ep', None, 'tp'), may hold values from -0.125 to 0.125
- down_weight: bfloat16 [8, 512, 2048], P('ep', None, 'tp'), may hold values from -0.25 to 0.25
Outputs:
- mixed: bfloat16 [8192, 2048], P(('grp', 'ep'), 'tp'), parts along dimension 0
There are 2 independent parts, one for each index of `grp`. A program takes and returns all parts, laid end to end along the dimension named above; an argument that names none is the same for every part. Nothing has to cross between parts.
Inputs may be any that keep to these rules, and one draw needn't show every extreme that they name: `expert_ids`: each token names 2 different experts. Among the 512 tokens of one index of ep (aligned blocks of rows) at most 192 name the same expert, and in some block some expert is named by exactly 192 of them.
All inputs are finite; a program needn't handle non-finite values.
Results may differ from a plain program's by a relative error of at most 0.007.
Values may be sent and summed in bfloat16 or wider, within the bound.
A program may use at most 64 MiB of HBM per device.

v0:
```python
import functools

import jax
import jax.numpy as jnp
from jax import lax
from jax.experimental import pallas as pl
from jax.experimental.pallas import tpu as pltpu
from jax.sharding import PartitionSpec as P

MESH = pl.DeviceIdType.MESH
COLS = 2
PARTS = 8
CUTS = 4


def normalize(rows, norm_gain):
    xf = rows.astype(jnp.float32)
    scale = lax.rsqrt(jnp.mean(xf * xf, axis=-1, keepdims=True) + 1e-06)
    return (xf * scale * norm_gain[None, :]).astype(jnp.bfloat16)


def sparse_form(tokens, norm_gain, expert_ids, route_weights, gate_weight, up_weight, down_weight):
    tok_rows, half = tokens.shape
    width = half * lax.axis_size("tp")
    experts = lax.axis_size("ep")
    top = expert_ids.shape[1]
    capacity = max(2, (3 * tok_rows * top + 2 * experts - 1) // (2 * experts))
    flat = expert_ids.reshape(-1)
    onehot = (flat[:, None] == jnp.arange(experts, dtype=jnp.int32)[None, :]).astype(jnp.int32)
    earlier = jnp.cumsum(onehot, axis=0) - onehot
    slot = jnp.sum(earlier * onehot, axis=-1)
    position = flat * capacity + slot
    owner = jnp.arange(flat.shape[0], dtype=jnp.int32) // top
    w_gate = gate_weight[0]
    w_up = up_weight[0]
    w_down = down_weight[0]
    send = jnp.zeros((experts * capacity, half), jnp.bfloat16).at[position].set(tokens[owner])
    send = send.reshape(experts, capacity, half)
    received = lax.all_to_all(send, "ep", split_axis=0, concat_axis=0, tiled=True)
    sources = received.shape[0]
    count = received.shape[1]
    whole_rows = lax.all_gather(received, "tp", axis=2, tiled=True)
    rows = normalize(whole_rows.reshape(sources * count, width), norm_gain)
    gate = jnp.dot(rows, w_gate, preferred_element_type=jnp.float32)
    upper = jnp.dot(rows, w_up, preferred_element_type=jnp.float32)
    hidden = (jax.nn.silu(gate) * upper).astype(jnp.bfloat16)
    result = jnp.dot(
        lax.all_gather(hidden, "tp", axis=1, tiled=True), w_down, preferred_element_type=jnp.float32
    )
    result = result.astype(jnp.bfloat16).reshape(sources, count, half)
    back = lax.all_to_all(result, "ep", split_axis=0, concat_axis=0, tiled=True)
    picked = back.reshape(experts * capacity, half)[position].astype(jnp.float32)
    picked = picked * route_weights.reshape(-1)[:, None]
    return jnp.sum(picked.reshape(tok_rows, top, half), axis=1).astype(jnp.bfloat16)


def line_kernel(
    length, tok_ref, gain_ref, route_ref, gate_in, up_in, down_in, out_ref,
    raw, x, wt, wg, wu, wd, hid, acc, part, from_low, from_high, fin, outs,
    swap_s, swap_r, loc, own_s, own_r, wy_s, wy_r, wx_s, wx_r, p1_s, p1_r, p2_s, p2_r,
    up_s, up_r, dn_s, dn_r, upt_s, upt_r, dnt_s, dnt_r, ru_s, ru_r, rd_s, rd_r, fin_s, fin_r,
):
    f32 = jnp.float32
    g, ep, c = lax.axis_index("grp"), lax.axis_index("ep"), lax.axis_index("tp")
    z, y = ep // COLS, ep % COLS
    last = length - 1
    mate, across, beside = {"tp": 1 - c}, {"grp": 1 - g}, {"ep": z * COLS + 1 - y}
    above, below = {"ep": ep + COLS}, {"ep": ep - COLS}
    rows, half = raw.shape[1], raw.shape[2]
    piece = rows // (PARTS // 2)

    def remote(src, dst, ss, rs, dev):
        return pltpu.make_async_remote_copy(
            src_ref=src, dst_ref=dst, send_sem=ss, recv_sem=rs, device_id=dev, device_id_type=MESH
        )

    barrier = pltpu.get_barrier_semaphore()
    for dev in (mate, across, beside):
        pl.semaphore_signal(barrier, inc=1, device_id=dev, device_id_type=MESH)

    @pl.when(z < last)
    def _():
        pl.semaphore_signal(barrier, inc=1, device_id=above, device_id_type=MESH)

    @pl.when(z > 0)
    def _():
        pl.semaphore_signal(barrier, inc=1, device_id=below, device_id_type=MESH)

    ends = jnp.where(z == 0, 1, 0) + jnp.where(z == last, 1, 0)
    pl.semaphore_wait(barrier, 5 - ends)

    swap = remote(tok_ref.at[1 - c], raw.at[c], swap_s, swap_r, mate)
    swap.start()

    mats = ((gate_in, wg), (up_in, wu), (down_in, wd))
    chunks = []
    for m in range(3):
        size = mats[m][0].shape[0] // (2 * CUTS)
        for u in range(CUTS):
            chunks.append((m, u, size))
    amount = len(chunks)

    def cut(portion, u, size):
        return pl.ds(pl.multiple_of((portion * CUTS + u) * size, size), size)

    def send_y(t):
        m, u, q = chunks[t]
        src, dst = mats[m]
        return remote(src.at[cut(g, u, q)], dst.at[1, c, cut(g, u, q)], wy_s.at[t], wy_r.at[t], beside)

    def send_x(t, portion):
        m, u, q = chunks[t]
        buf = mats[m][1].at[1, c, cut(portion, u, q)]
        return remote(buf, buf, wx_s.at[t], wx_r.at[t], across)

    def send_mate(t, portion, half_of, ss, rs):
        m, u, q = chunks[t]
        buf = mats[m][1].at[1, half_of, cut(portion, u, q)]
        return remote(buf, buf, ss.at[t], rs.at[t], mate)

    for t in range(amount):
        send_y(t).start()
    own = []
    for m in range(3):
        src, dst = mats[m]
        own.append(remote(src, dst.at[0, c], own_s.at[m], own_r.at[m], mate))
    local = [pltpu.make_async_copy(mats[m][0], mats[m][1].at[0, c], loc.at[m]) for m in range(3)]

    for copy in own + local:
        copy.start()
    wt[z] = route_ref[...]
    swap.wait_recv()
    step = rows // 8

    def norm(i, carry):
        at = pl.ds(pl.multiple_of(i * step, step), step)
        a = tok_ref[c, at].astype(f32)
        b = raw[1 - c, at].astype(f32)
        total = jnp.sum(a * a, axis=-1, keepdims=True) + jnp.sum(b * b, axis=-1, keepdims=True)
        scale = lax.rsqrt(total / (2 * half) + 1e-06)
        x[z, c, at] = (a * scale * gain_ref[c]).astype(x.dtype)
        x[z, 1 - c, at] = (b * scale * gain_ref[1 - c]).astype(x.dtype)
        return carry

    lax.fori_loop(0, 8, norm, 0)

    def rise(b):
        return (
            remote(x.at[b], x.at[b], up_s.at[b], up_r.at[b], above),
            remote(wt.at[b], wt.at[b], upt_s.at[b], upt_r.at[b], above),
        )

    def fall(b):
        return (
            remote(x.at[b], x.at[b], dn_s.at[b], dn_r.at[b], below),
            remote(wt.at[b], wt.at[b], dnt_s.at[b], dnt_r.at[b], below),
        )

    @pl.when(z < last)
    def _():
        for copy in rise(z):
            copy.start()

    @pl.when(z > 0)
    def _():
        for copy in fall(z):
            copy.start()

    def hand_on(k):
        @pl.when(z >= k)
        def _():
            for copy in rise(z - k):
                copy.wait_recv()

            @pl.when(z < last)
            def _():
                for copy in rise(z - k):
                    copy.start()

        @pl.when(z + k <= last)
        def _():
            for copy in fall(z + k):
                copy.wait_recv()

            @pl.when(z > 0)
            def _():
                for copy in fall(z + k):
                    copy.start()

    def got_y(t):
        m, u, q = chunks[t]
        send_y(t).wait_recv()
        send_x(t, g).start()
        send_mate(t, g, c, p1_s, p1_r).start()

    def got_x(t):
        send_x(t, 1 - g).wait_recv()
        send_mate(t, 1 - g, c, p2_s, p2_r).start()

    for t in range(amount):
        got_y(t)
        if t >= 1:
            got_x(t - 1)
        if t == 3 * amount // 4 - 1:
            hand_on(1)
    got_x(amount - 1)
    for t in range(amount):
        send_mate(t, g, 1 - c, p1_s, p1_r).wait_recv()
        send_mate(t, 1 - g, 1 - c, p2_s, p2_r).wait_recv()
    for m in range(3):
        local[m].wait()
        own[m].wait_recv()

    def experts_on(b):
        columns = wt[b].T
        lane = lax.broadcasted_iota(jnp.int32, columns.shape, 1)
        for s in range(2):
            expert = z * COLS + (y if s == 0 else 1 - y)
            weight = jnp.sum(jnp.where(lane == expert, columns, 0.0), axis=1, keepdims=True)
            for h in range(2):
                both = []
                for w in (wg, wu):
                    both.append(
                        jnp.dot(x[b, 0], w[s, h, :half], preferred_element_type=f32)
                        + jnp.dot(x[b, 1], w[s, h, half:], preferred_element_type=f32)
                    )
                gate, upper = both
                silu = gate * (0.5 * (1.0 + jnp.tanh(0.5 * gate)))
                wide = gate.shape[1]
                hid[:, h * wide:(h + 1) * wide] = (silu * upper).astype(hid.dtype)
            for f in range(2):
                got = jnp.dot(hid[...], wd[s, f], preferred_element_type=f32)
                got = got.astype(jnp.bfloat16).astype(f32) * weight
                if s == 0:
                    acc[f] = got
                else:
                    got = acc[f] + got
                    acc[f] = got
                    part[b, f] = got.astype(part.dtype)

    def place(j):
        return (1 - c if j < PARTS // 2 else c), pl.ds((j % (PARTS // 2)) * piece, piece)

    def sum_up(b, j):
        f, at = place(j)
        return remote(part.at[b, f, at], from_low.at[b, f, at], ru_s.at[b, j], ru_r.at[b, j], above)

    def sum_down(b, j):
        f, at = place(j)
        return remote(part.at[b, f, at], from_high.at[b, f, at], rd_s.at[b, j], rd_r.at[b, j], below)

    def wave_up(b, j, side):
        f, at = place(j)

        @pl.when(side & (z < b) & (b <= last))
        def _():
            @pl.when(z > 0)
            def _():
                sum_up(b, j).wait_recv()
                part[b, f, at] = (part[b, f, at].astype(f32) + from_low[b, f, at].astype(f32)).astype(part.dtype)
            sum_up(b, j).start()

    def wave_down(b, j, side):
        f, at = place(j)

        @pl.when(side & (z > b) & (b >= 0))
        def _():
            @pl.when(z < last)
            def _():
                sum_down(b, j).wait_recv()
                part[b, f, at] = (part[b, f, at].astype(f32) + from_high[b, f, at].astype(f32)).astype(part.dtype)
            sum_down(b, j).start()

    def stage(k, carry):
        @pl.when(k > 1)
        def _():
            hand_on(k)

        def one(i, inner):
            b = jnp.where(k > last, z, jnp.where(i == 0, z - k, z + k))

            @pl.when((b >= 0) & (b <= last) & ((k <= last) | (i == 0)))
            def _():
                experts_on(b)
            return inner

        lax.fori_loop(0, 2, one, 0)

        for j in range(PARTS + 1):
            if j < PARTS:
                wave_up(k, j, z < length // 2)
                wave_down(last - k, j, z >= length // 2)
            if j > 0:
                wave_down(last - k, j - 1, z < length // 2)
                wave_up(k, j - 1, z >= length // 2)
        return carry

    lax.fori_loop(1, length + 1, stage, 0)

    def give(r):
        at = pl.ds(r * piece, piece)
        return remote(fin.at[at], outs.at[c, at], fin_s.at[r], fin_r.at[r], mate)

    for j in range(PARTS):
        f, at = place(j)

        @pl.when(z > 0)
        def _():
            sum_up(z, j).wait_recv()
            acc[f, at] = acc[f, at] + from_low[z, f, at].astype(f32)

        @pl.when(z < last)
        def _():
            sum_down(z, j).wait_recv()
            acc[f, at] = acc[f, at] + from_high[z, f, at].astype(f32)

        if j < PARTS // 2:
            fin[at] = acc[f, at].astype(fin.dtype)
            give(j).start()
        else:
            out_ref[c, at] = acc[f, at].astype(out_ref.dtype)
    for r in range(PARTS // 2):
        at = pl.ds(r * piece, piece)
        give(r).wait_recv()
        out_ref[1 - c, at] = outs[1 - c, at]

    swap.wait_send()
    for copy in own:
        copy.wait_send()
    for t in range(amount):
        send_y(t).wait_send()
        send_x(t, g).wait_send()
        send_mate(t, g, c, p1_s, p1_r).wait_send()
        send_mate(t, 1 - g, c, p2_s, p2_r).wait_send()
    for r in range(PARTS // 2):
        give(r).wait_send()
    for b in range(length):
        @pl.when((z >= b) & (z < last))
        def _():
            for copy in rise(b):
                copy.wait_send()

        @pl.when((z <= b) & (z > 0))
        def _():
            for copy in fall(b):
                copy.wait_send()

        @pl.when(z < b)
        def _():
            for j in range(PARTS):
                sum_up(b, j).wait_send()

        @pl.when(z > b)
        def _():
            for j in range(PARTS):
                sum_down(b, j).wait_send()


def line_form(tokens, norm_gain, expert_ids, route_weights, gate_weight, up_weight, down_weight):
    tok_rows, half = tokens.shape
    experts = lax.axis_size("ep")
    length = experts // COLS
    rows = tok_rows // 2
    mine = lax.axis_index("tp")
    bf16, f32 = jnp.bfloat16, jnp.float32
    chosen = expert_ids[None] == jnp.arange(experts, dtype=jnp.int32)[:, None, None]
    route = jnp.sum(jnp.where(chosen, route_weights[None], 0.0), axis=-1)
    route = lax.dynamic_slice_in_dim(route, mine * rows, rows, axis=1)
    gate, up, down = gate_weight[0], up_weight[0], down_weight[0]
    dma, vmem = pltpu.SemaphoreType.DMA, pltpu.VMEM
    block = (length, 2, rows, half)
    cuts, sums = (3 * CUTS,), (length, PARTS)
    sems = []
    for shape in (
        (1,), (3,), cuts, cuts, cuts, cuts, (length,), (length,), (length,), (length,), sums, sums, (PARTS // 2,)
    ):
        sems += [dma(shape), dma(shape)]
    sems = [dma, dma, dma((3,))] + sems[2:]
    out = pl.pallas_call(
        functools.partial(line_kernel, length),
        out_shape=jax.ShapeDtypeStruct((2, rows, half), bf16),
        in_specs=[pl.BlockSpec(memory_space=vmem)] * 3 + [pl.BlockSpec(memory_space=pl.ANY)] * 3,
        out_specs=pl.BlockSpec(memory_space=vmem),
        scratch_shapes=[
            vmem((2, rows, half), bf16),
            vmem(block, bf16),
            vmem((length, experts, rows), f32),
            vmem((2, 2) + gate.shape, bf16),
            vmem((2, 2) + up.shape, bf16),
            vmem((2, 2) + down.shape, bf16),
            vmem((rows, 2 * gate.shape[1]), bf16),
            vmem((2, rows, half), f32),
            vmem(block, bf16),
            vmem(block, bf16),
            vmem(block, bf16),
            vmem((rows, half), bf16),
            vmem((2, rows, half), bf16),
        ]
        + sems,
        compiler_params=pltpu.CompilerParams(
            collective_id=0, has_side_effects=True, vmem_limit_bytes=60 * 1024 * 1024
        ),
    )(tokens.reshape(2, rows, half), norm_gain.reshape(2, 1, half), route, gate, up, down)
    return out.reshape(tok_rows, half)


def solution(mesh):
    in_specs = (
        P(("grp", "ep"), "tp"),
        P(),
        P(("grp", "ep"), None),
        P(("grp", "ep"), None),
        P("ep", None, "tp"),
        P("ep", None, "tp"),
        P("ep", None, "tp"),
    )
    out_specs = P(("grp", "ep"), "tp")
    shape = mesh.shape

    def on_device(tokens, norm_gain, expert_ids, *rest):
        dense = shape["ep"] <= 4 * expert_ids.shape[1] and shape["ep"] % COLS == 0 and shape["ep"] > COLS
        form = line_form if dense and shape["grp"] == 2 and shape["tp"] == 2 else sparse_form
        return form(tokens, norm_gain, expert_ids, *rest)

    return jax.shard_map(
        on_device, mesh=mesh, in_specs=in_specs, out_specs=out_specs, check_vma=False
    )
```

profile of v0, /device:TPU:8, one launch (start us, length us, event | category | flops | bytes accessed | tf_op | source)
XLA Modules:
  0.0 135.4 jit_solution(9823071714552479036)
XLA Ops:
  0.0 0.0 copy-start.1
  0.0 0.0 copy-start
  0.0 0.7 copy-done.1
  0.7 0.0 copy-done
  0.7 0.6 constant_dynamic-slice_fusion.route_ref
  1.3 131.8 %shard_map.73 = bf16[2,256,1024]{2,1,0:T(8,128)(2,1)} custom-call(bf16[2,256,1024]{2,1,0:T(8,128)(2,1)} %bitcast.7, f32[2,1,1024]{2,1,0:T(1,128)} %bitcast.11, f32[8,256]{1,0:T(8,128)} %constant_dynamic-slice_fusion.route_ref, bf16[2048,256]{1,0:T(8,128)(2,1)} %bitcast.8, bf16[2048,256]{1,0:T(8,128)(2,1)} %bitcast.9, bf16[512,1024]{1,0:T(8,128)(2,1)} %bitcast.10), custom_call_target="tpu_custom_call" | custom-call | tf_op jit(solution)/shard_map/pallas_call | solution.py:379
  133.1 2.3 %copy.11 = bf16[512,1024]{1,0:T(8,128)(2,1)} copy(bf16[512,1024]{1,0:T(8,128)(2,1)} %bitcast.6) | data formatting | bytes 2097152
  (1 shorter events, 0.0 us)
Async XLA Ops:
  0.0 0.7 copy-start.1
  0.0 0.7 copy-start
where the time goes:
time: 137 us; the launch traced here: 135 us
  Pallas kernels  132 us (96%)
  local copies, waits for them, and re-layouts  3.57 us (3%)
    pallas_call x1, Pallas kernels, line_form(): pl.pallas_call(functools.partial(line_kernel, length), out_shape=jax.Shap...  132 us
    unnamed x5, local copies, waits for them, and re-layouts  2.96 us

commit v1 on v0

v1 whole, which is shorter than its diff:
```python
import functools

import jax
import jax.numpy as jnp
from jax import lax
from jax.experimental import pallas as pl
from jax.experimental.pallas import tpu as pltpu
from jax.sharding import PartitionSpec as P

MESH = pl.DeviceIdType.MESH
COLS = 2
PIECES = 8
LEAD = 2
CUTS = 4


def normalize(rows, norm_gain):
    xf = rows.astype(jnp.float32)
    scale = lax.rsqrt(jnp.mean(xf * xf, axis=-1, keepdims=True) + 1e-06)
    return (xf * scale * norm_gain[None, :]).astype(jnp.bfloat16)


def sparse_form(tokens, norm_gain, expert_ids, route_weights, gate_weight, up_weight, down_weight):
    tok_rows, half = tokens.shape
    width = half * lax.axis_size("tp")
    experts = lax.axis_size("ep")
    top = expert_ids.shape[1]
    capacity = max(2, (3 * tok_rows * top + 2 * experts - 1) // (2 * experts))
    flat = expert_ids.reshape(-1)
    onehot = (flat[:, None] == jnp.arange(experts, dtype=jnp.int32)[None, :]).astype(jnp.int32)
    earlier = jnp.cumsum(onehot, axis=0) - onehot
    slot = jnp.sum(earlier * onehot, axis=-1)
    position = flat * capacity + slot
    owner = jnp.arange(flat.shape[0], dtype=jnp.int32) // top
    w_gate = gate_weight[0]
    w_up = up_weight[0]
    w_down = down_weight[0]
    send = jnp.zeros((experts * capacity, half), jnp.bfloat16).at[position].set(tokens[owner])
    send = send.reshape(experts, capacity, half)
    received = lax.all_to_all(send, "ep", split_axis=0, concat_axis=0, tiled=True)
    sources = received.shape[0]
    count = received.shape[1]
    whole_rows = lax.all_gather(received, "tp", axis=2, tiled=True)
    rows = normalize(whole_rows.reshape(sources * count, width), norm_gain)
    gate = jnp.dot(rows, w_gate, preferred_element_type=jnp.float32)
    upper = jnp.dot(rows, w_up, preferred_element_type=jnp.float32)
    hidden = (jax.nn.silu(gate) * upper).astype(jnp.bfloat16)
    result = jnp.dot(
        lax.all_gather(hidden, "tp", axis=1, tiled=True), w_down, preferred_element_type=jnp.float32
    )
    result = result.astype(jnp.bfloat16).reshape(sources, count, half)
    back = lax.all_to_all(result, "ep", split_axis=0, concat_axis=0, tiled=True)
    picked = back.reshape(experts * capacity, half)[position].astype(jnp.float32)
    picked = picked * route_weights.reshape(-1)[:, None]
    return jnp.sum(picked.reshape(tok_rows, top, half), axis=1).astype(jnp.bfloat16)


def line_kernel(
    length, cap, tok_ref, gain_ref, route_ref, gate_in, up_in, down_in, out_ref,
    raw, x, wt, wg, wu, wd, hid, part, came, slim, slim_in, acc,
    swap_s, swap_r, loc, wy_s, wy_r, wx_s, wx_r, gat_s, gat_r, tab_s, tab_r,
    half_s, half_r, hid_s, hid_r, sum_s, sum_r, slim_s, slim_r,
):
    f32, bf16 = jnp.float32, jnp.bfloat16
    g, ep, c = lax.axis_index("grp"), lax.axis_index("ep"), lax.axis_index("tp")
    z, y = ep // COLS, ep % COLS
    last = length - 1
    flip = z >= length // 2
    end = jnp.where(flip, last, 0)
    mid = jnp.where(flip, last - 1, 1)
    far_mid, far_end = last - mid, last - end
    outer, inner = z == end, z == mid
    mate, across, beside = {"tp": 1 - c}, {"grp": 1 - g}, {"ep": z * COLS + 1 - y}
    to_end, to_mid, to_far = {"ep": end * COLS + y}, {"ep": mid * COLS + y}, {"ep": far_mid * COLS + y}
    rows, half = raw.shape
    piece = rows // PIECES
    unit = rows // 2
    per_unit = PIECES // 2
    wide = hid.shape[3]

    def remote(src, dst, ss, rs, dev):
        return pltpu.make_async_remote_copy(
            src_ref=src, dst_ref=dst, send_sem=ss, recv_sem=rs, device_id=dev, device_id_type=MESH
        )

    def span(q):
        return pl.ds(q * piece if isinstance(q, int) else pl.multiple_of(q * piece, piece), piece)

    barrier = pltpu.get_barrier_semaphore()
    for dev in (mate, across, beside):
        pl.semaphore_signal(barrier, inc=1, device_id=dev, device_id_type=MESH)

    @pl.when(outer)
    def _():
        pl.semaphore_signal(barrier, inc=1, device_id=to_mid, device_id_type=MESH)

    @pl.when(inner)
    def _():
        pl.semaphore_signal(barrier, inc=1, device_id=to_end, device_id_type=MESH)
        pl.semaphore_signal(barrier, inc=1, device_id=to_far, device_id_type=MESH)

    pl.semaphore_wait(barrier, jnp.where(outer, 4, 5))

    def swap(q):
        return remote(tok_ref.at[span(q)], raw.at[span(q)], swap_s.at[q], swap_r.at[q], mate)

    for q in range(PIECES):
        swap(q).start()

    mats = ((gate_in, wg), (up_in, wu), (down_in, wd))
    chunks = []
    for m in range(3):
        size = mats[m][0].shape[0] // (2 * CUTS)
        for u in range(CUTS):
            chunks.append((m, u, size))
    amount = len(chunks)

    def cut(portion, u, size):
        return pl.ds(pl.multiple_of((portion * CUTS + u) * size, size), size)

    def send_y(t):
        m, u, q = chunks[t]
        src, dst = mats[m]
        return remote(src.at[cut(g, u, q)], dst.at[1, cut(g, u, q)], wy_s.at[t], wy_r.at[t], beside)

    def send_x(t, portion):
        m, u, q = chunks[t]
        buf = mats[m][1].at[1, cut(portion, u, q)]
        return remote(buf, buf, wx_s.at[t], wx_r.at[t], across)

    for t in range(amount):
        send_y(t).start()
    local = [pltpu.make_async_copy(mats[m][0], mats[m][1].at[0], loc.at[m]) for m in range(3)]
    for copy in local:
        copy.start()

    def gather(b, q, way, dev):
        at = x.at[b, c, span(q)]
        return remote(at, at, gat_s.at[way, b, q], gat_r.at[b, q], dev)

    def table(b, way, dev, src=None):
        src = wt.at[b] if src is None else src
        return remote(src, wt.at[b], tab_s.at[way, b], tab_r.at[b], dev)

    def share(b, q, side):
        at = x.at[b, side, span(q)]
        return remote(at, at, half_s.at[b, q], half_r.at[b, q], mate)

    def total(b, q, dev):
        return remote(part.at[b, span(q)], came.at[b, span(q)], sum_s.at[b, q], sum_r.at[b, q], dev)

    def compact(s, dev):
        return remote(slim.at[s], slim_in.at[s], slim_s.at[s], slim_r.at[s], dev)

    def hand(slot, side, count):
        at = hid.at[slot, side, pl.ds(0, count)]
        return remote(at, at, hid_s.at[slot], hid_r.at[slot], mate)

    @pl.when(outer)
    def _():
        table(z, 0, to_mid, route_ref).start()

    @pl.when(inner)
    def _():
        table(z, 0, to_end, route_ref).start()
        table(z, 1, to_far, route_ref).start()

    wt[z] = route_ref[...]

    def norm(q, carry):
        swap(q).wait_recv()
        at = span(q)
        a = tok_ref[at].astype(f32)
        b = raw[at].astype(f32)
        total_sq = jnp.sum(a * a, axis=-1, keepdims=True) + jnp.sum(b * b, axis=-1, keepdims=True)
        scale = lax.rsqrt(total_sq / (2 * half) + 1e-06)
        x[z, c, at] = (a * scale * gain_ref[c]).astype(bf16)
        x[z, 1 - c, at] = (b * scale * gain_ref[1 - c]).astype(bf16)

        @pl.when(outer)
        def _():
            gather(z, q, 0, to_mid).start()

        @pl.when(inner)
        def _():
            gather(z, q, 0, to_end).start()

            @pl.when(q < LEAD)
            def _():
                gather(z, q, 1, to_far).start()
        return carry

    lax.fori_loop(0, PIECES, norm, 0)

    def got_y(t):
        send_y(t).wait_recv()
        send_x(t, g).start()

    def outer_stream(j):
        b = (mid, far_end, far_mid)[j // PIECES]
        q = j % PIECES
        gather(b, q, 0, to_mid).wait_recv()
        share(b, q, c).start()

    def inner_stream(j):
        if j < LEAD:
            b, q = far_mid, j
        elif j < LEAD + PIECES:
            b, q = far_end, j - LEAD
        else:
            b, q = far_mid, j - PIECES
        gather(b, q, 1, to_far).wait_recv()
        share(b, q, c).start()
        if j >= LEAD:
            gather(b, q, 0, to_end).start()
        if j == LEAD + PIECES - 1:
            for early in range(LEAD):
                gather(far_mid, early, 0, to_end).start()

    def inner_end(q):
        gather(end, q, 0, to_end).wait_recv()
        share(end, q, c).start()
        gather(end, q, 1, to_far).start()
        if q == PIECES - 1:
            for late in range(LEAD, PIECES):
                gather(z, late, 1, to_far).start()

    def pick(table_rows, e):
        lane = lax.broadcasted_iota(jnp.int32, table_rows.shape, 0)
        return jnp.sum(jnp.where(lane == e, table_rows, 0.0), axis=0, keepdims=True)

    def selection(b, e):
        weights = wt[b]
        chosen = jnp.where(weights > 0.0, 1.0, 0.0)
        above = lax.broadcasted_iota(jnp.int32, (rows, rows), 0)
        along = lax.broadcasted_iota(jnp.int32, (rows, rows), 1)
        before = jnp.where(above < along, 1.0, 0.0).astype(bf16)
        rank = jnp.dot(chosen.astype(bf16), before, preferred_element_type=f32)
        place = pick(jnp.where(chosen > 0.0, rank, -1.0), e)
        slot = lax.broadcasted_iota(jnp.int32, (cap, rows), 0).astype(f32)
        return jnp.where(slot == place, 1.0, 0.0), pick(weights, e)

    def hidden_half(first, second, s):
        both = []
        for w in (wg, wu):
            both.append(
                jnp.dot(first, w[s, :half], preferred_element_type=f32)
                + jnp.dot(second, w[s, half:], preferred_element_type=f32)
            )
        gate, upper = both
        return (gate * (0.5 * (1.0 + jnp.tanh(0.5 * gate))) * upper).astype(bf16)

    def lowered(slot, s, count):
        at = pl.ds(0, count)
        return jnp.dot(hid[slot, 0, at], wd[s, :wide], preferred_element_type=f32) + jnp.dot(
            hid[slot, 1, at], wd[s, wide:], preferred_element_type=f32
        )

    def slim_rows(s):
        slot = 4 * length + s
        mark, weight_row = selection(mid, end * COLS + (y if s == 0 else 1 - y))
        ones = mark.astype(bf16)
        first = jnp.dot(ones, x[mid, 0], preferred_element_type=f32).astype(bf16)
        second = jnp.dot(ones, x[mid, 1], preferred_element_type=f32).astype(bf16)
        hid[slot, c, pl.ds(0, cap)] = hidden_half(first, second, s)
        hand(slot, c, cap).start()
        weight = jnp.sum(mark * weight_row, axis=1, keepdims=True)
        hand(slot, 1 - c, cap).wait_recv()
        slim[s] = (lowered(slot, s, cap) * weight).astype(bf16)
        compact(s, to_mid).start()

    def widen(s, at):
        mark, _ = selection(mid, end * COLS + (y if s == 0 else 1 - y))
        ones = mark.astype(bf16)
        return lax.dot_general(ones, slim_in[s], (((0,), (0,)), ((), ())), preferred_element_type=f32)

    def dense_unit(b, part_of, slot):
        at = pl.ds(pl.multiple_of(part_of * unit, unit), unit)
        columns = wt[b, :, at].T
        lane = lax.broadcasted_iota(jnp.int32, columns.shape, 1)
        first, second = x[b, 0, at], x[b, 1, at]
        for s in range(2):
            hid[slot + s, c] = hidden_half(first, second, s)
            hand(slot + s, c, unit).start()
        sums = None
        for s in range(2):
            expert = z * COLS + (y if s == 0 else 1 - y)
            weight = jnp.sum(jnp.where(lane == expert, columns, 0.0), axis=1, keepdims=True)
            hand(slot + s, 1 - c, unit).wait_recv()
            got = lowered(slot + s, s, unit) * weight
            sums = got if sums is None else sums + got

        @pl.when(b == z)
        def _():
            acc[at] = sums

        @pl.when(b != z)
        def _():
            part[b, at] = sums.astype(bf16)

    def pass_on(b, q, dev):
        total(b, q, dev).wait_recv()
        at = span(q)
        part[b, at] = (part[b, at].astype(f32) + came[b, at].astype(f32)).astype(bf16)
        total(b, q, dev).start()

    def take_in(q):
        total(z, q, to_far).wait_recv()
        at = span(q)
        acc[at] = acc[at] + came[z, at].astype(f32)

    @pl.when(outer)
    def _():
        table(mid, 0, to_mid).wait_recv()
        for j in range(amount):
            outer_stream(j)
            got_y(j)
            if j == PIECES + 1:
                for q in range(PIECES):
                    share(mid, q, 1 - c).wait_recv()
                for m in range(3):
                    local[m].wait()
                slim_rows(0)
        table(far_end, 0, to_mid).wait_recv()
        table(far_mid, 0, to_mid).wait_recv()

    @pl.when(inner)
    def _():
        table(end, 0, to_end).wait_recv()
        table(end, 1, to_far).start()
        table(far_mid, 1, to_far).wait_recv()
        table(far_mid, 0, to_end).start()
        for j in range(amount):
            if j < PIECES:
                inner_end(j)
            inner_stream(j)
            got_y(j)
            if j == PIECES:
                table(far_end, 1, to_far).wait_recv()
                table(far_end, 0, to_end).start()
        for m in range(3):
            local[m].wait()

    for t in range(amount):
        send_x(t, 1 - g).wait_recv()

    def step(i, carry):
        k, part_of = i // 2, i % 2
        b = jnp.where(k == 0, far_end, jnp.where(k == 1, end, jnp.where(k == 2, far_mid, mid)))

        @pl.when(outer)
        def _():
            for n in range(2):
                @pl.when(i == n)
                def _():
                    for q in range(n * per_unit, (n + 1) * per_unit):
                        if PIECES + q >= amount:
                            outer_stream(PIECES + q)
                    for q in range(n * per_unit, (n + 1) * per_unit):
                        share(far_end, q, 1 - c).wait_recv()

                @pl.when(i == 4 + n)
                def _():
                    for q in range(n * per_unit, (n + 1) * per_unit):
                        outer_stream(2 * PIECES + q)
                    for q in range(n * per_unit, (n + 1) * per_unit):
                        share(far_mid, q, 1 - c).wait_recv()

            @pl.when(i == 6)
            def _():
                slim_rows(1)

        @pl.when(inner)
        def _():
            rest = 2 * PIECES - amount
            for n in range(2):
                @pl.when(i == n)
                def _():
                    for q in range(n * per_unit, (n + 1) * per_unit):
                        share(far_end, q, 1 - c).wait_recv()

                @pl.when(i == 2 + n)
                def _():
                    for j in range(amount + n * rest // 2, amount + (n + 1) * rest // 2):
                        inner_stream(j)
                    for q in range(n * per_unit, (n + 1) * per_unit):
                        share(end, q, 1 - c).wait_recv()

                @pl.when(i == 4 + n)
                def _():
                    for q in range(n * per_unit, (n + 1) * per_unit):
                        share(far_mid, q, 1 - c).wait_recv()
            for n in range(4):
                @pl.when(i == 4 + n)
                def _():
                    for q in range(n * PIECES // 4, (n + 1) * PIECES // 4):
                        pass_on(far_end, q, to_far)
                    if n >= 2:
                        for q in range((n - 2) * PIECES // 4, (n - 1) * PIECES // 4):
                            pass_on(end, q, to_end)

        @pl.when(inner | (k < 3))
        def _():
            dense_unit(b, part_of, 2 * i)

        @pl.when(outer & ((k == 0) | (k == 2)))
        def _():
            for n in range(per_unit):
                total(b, part_of * per_unit + n, to_mid).start()
        return carry

    lax.fori_loop(0, 2 * length, step, 0)

    @pl.when(outer)
    def _():
        for q in range(PIECES):
            total(z, q, to_mid).wait_recv()
            at = span(q)
            out_ref[at] = (acc[at] + came[z, at].astype(f32)).astype(bf16)

    @pl.when(inner)
    def _():
        compact(0, to_end).wait_recv()
        acc[...] = acc[...] + widen(0, None)
        for q in range(PIECES // 2, PIECES):
            pass_on(end, q, to_end)
        for q in range(PIECES):
            pass_on(far_mid, q, to_far)
            if q >= 2:
                take_in(q - 2)
        for q in range(PIECES - 2, PIECES):
            take_in(q)
        compact(1, to_end).wait_recv()
        out_ref[...] = (acc[...] + widen(1, None)).astype(bf16)

    for q in range(PIECES):
        swap(q).wait_send()
    for t in range(amount):
        send_y(t).wait_send()
        send_x(t, g).wait_send()

    @pl.when(outer)
    def _():
        table(z, 0, to_mid, route_ref).wait_send()
        for s in range(2):
            compact(s, to_mid).wait_send()
            hand(4 * length + s, c, cap).wait_send()
        for slot in range(4 * length - 4):
            hand(slot, c, unit).wait_send()
        for q in range(PIECES):
            gather(z, q, 0, to_mid).wait_send()
            for b in (far_end, far_mid):
                total(b, q, to_mid).wait_send()
            for b in (mid, far_end, far_mid):
                share(b, q, c).wait_send()

    @pl.when(inner)
    def _():
        for slot in range(4 * length):
            hand(slot, c, unit).wait_send()
        table(z, 0, to_end, route_ref).wait_send()
        table(z, 1, to_far, route_ref).wait_send()
        table(end, 1, to_far).wait_send()
        table(far_mid, 0, to_end).wait_send()
        table(far_end, 0, to_end).wait_send()
        for q in range(PIECES):
            for b in (z, far_mid, far_end):
                gather(b, q, 0, to_end).wait_send()
            for b in (z, end):
                gather(b, q, 1, to_far).wait_send()
            total(end, q, to_end).wait_send()
            for b in (far_mid, far_end):
                total(b, q, to_far).wait_send()
            for b in (end, far_mid, far_end):
                share(b, q, c).wait_send()


def line_form(tokens, norm_gain, expert_ids, route_weights, gate_weight, up_weight, down_weight):
    tok_rows, half = tokens.shape
    experts = lax.axis_size("ep")
    length = experts // COLS
    top = expert_ids.shape[1]
    cap = (3 * tok_rows * top + 2 * experts - 1) // (2 * experts)
    bf16, f32 = jnp.bfloat16, jnp.float32
    chosen = expert_ids[None] == jnp.arange(experts, dtype=jnp.int32)[:, None, None]
    route = jnp.sum(jnp.where(chosen, route_weights[None], 0.0), axis=-1)
    gate, up, down = gate_weight[0], up_weight[0], down_weight[0]
    dma, vmem = pltpu.SemaphoreType.DMA, pltpu.VMEM
    block = (length, tok_rows, half)
    slots = 4 * length + 2
    cuts, bits = (3 * CUTS,), (length, PIECES)
    sems = [dma((PIECES,)), dma((PIECES,)), dma((3,))]
    for send, recv in (
        (cuts, cuts), (cuts, cuts), ((2,) + bits, bits), ((2, length), (length,)),
        (bits, bits), ((slots,), (slots,)), (bits, bits), ((2,), (2,)),
    ):
        sems += [dma(send), dma(recv)]
    return pl.pallas_call(
        functools.partial(line_kernel, length, cap),
        out_shape=jax.ShapeDtypeStruct((tok_rows, half), bf16),
        in_specs=[pl.BlockSpec(memory_space=vmem)] * 3 + [pl.BlockSpec(memory_space=pl.ANY)] * 3,
        out_specs=pl.BlockSpec(memory_space=vmem),
        scratch_shapes=[
            vmem((tok_rows, half), bf16),
            vmem((length, 2, tok_rows, half), bf16),
            vmem((length, experts, tok_rows), f32),
            vmem((2,) + gate.shape, bf16),
            vmem((2,) + up.shape, bf16),
            vmem((2,) + down.shape, bf16),
            vmem((slots, 2, tok_rows // 2, gate.shape[1]), bf16),
            vmem(block, bf16),
            vmem(block, bf16),
            vmem((2, cap, half), bf16),
            vmem((2, cap, half), bf16),
            vmem((tok_rows, half), f32),
        ]
        + sems,
        compiler_params=pltpu.CompilerParams(
            collective_id=0, has_side_effects=True, vmem_limit_bytes=60 * 1024 * 1024
        ),
    )(tokens, norm_gain.reshape(2, 1, half), route, gate, up, down)


def solution(mesh):
    in_specs = (
        P(("grp", "ep"), "tp"),
        P(),
        P(("grp", "ep"), None),
        P(("grp", "ep"), None),
        P("ep", None, "tp"),
        P("ep", None, "tp"),
        P("ep", None, "tp"),
    )
    out_specs = P(("grp", "ep"), "tp")
    shape = mesh.shape

    def on_device(tokens, norm_gain, expert_ids, *rest):
        dense = shape["ep"] == 4 * COLS and shape["ep"] == 4 * expert_ids.shape[1]
        form = line_form if dense and shape["grp"] == 2 and shape["tp"] == 2 else sparse_form
        return form(tokens, norm_gain, expert_ids, *rest)

    return jax.shard_map(
        on_device, mesh=mesh, in_specs=in_specs, out_specs=out_specs, check_vma=False
    )
```

time: 137 us -> 117 us (0.85)
  Pallas kernels: 132 us -> 112 us
    pallas_call x1, Pallas kernels: 132 us -> 112 us  [line_form(): pl.pallas_call(functools.partial(line_kernel, length, cap), out_shape=jax...]
    unnamed x5 -> x3, local copies, waits for them, and re-layouts: 2.96 us -> 2.95 us
where the time goes in v1:
time: 117 us; the launch traced here: 116 us
  Pallas kernels  112 us (96%)
  local copies, waits for them, and re-layouts  2.95 us (3%)
  other arithmetic  1.3 us (1%)
    pallas_call x1, Pallas kernels, line_form(): pl.pallas_call(functools.partial(line_kernel, length, cap), out_shape=jax...  112 us
    unnamed x3, local copies, waits for them, and re-layouts  2.95 us

profile of v1, /device:TPU:8, one launch (start us, length us, event | category | flops | bytes accessed | tf_op | source)
XLA Modules:
  0.0 116.5 jit_solution(3021373873892684100)
XLA Ops:
  0.0 0.0 copy-start
  0.0 0.7 copy-done
  0.7 1.3 %select_reduce_fusion.route_ref = f32[8,512]{1,0:T(8,128)} fusion(f32[512,2]{0,1:T(2,128)S(1)} %copy-done, s32[512,2]{0,1:T(2,128)} %param.9), kind=kLoop, calls=%fused_computation | loop fusion | flops 20480 | bytes 24576 | tf_op jit(solution)/shard_map/reduce_sum | solution.py:486
  2.0 112.2 %shard_map.73 = bf16[512,1024]{1,0:T(8,128)(2,1)} custom-call(bf16[512,1024]{1,0:T(8,128)(2,1)} %tok_ref.1, f32[2,1,1024]{2,1,0:T(1,128)} %bitcast.7, f32[8,512]{1,0:T(8,128)} %select_reduce_fusion.route_ref, bf16[2048,256]{1,0:T(8,128)(2,1)} %bitcast.4, bf16[2048,256]{1,0:T(8,128)(2,1)} %bitcast.5, bf16[512,1024]{1,0:T(8,128)(2,1)} %bitcast.6), custom_call_target="tpu_custom_call" | custom-call | tf_op jit(solution)/shard_map/pallas_call | solution.py:498
  114.2 2.3 %copy.11 = bf16[512,1024]{1,0:T(8,128)(2,1)} copy(bf16[512,1024]{1,0:T(8,128)(2,1)} %shard_map.73) | data formatting | bytes 2097152
Async XLA Ops:
  0.0 0.7 copy-start

commit v2 on v1

v2 whole, which is shorter than its diff:
```python
import functools

import jax
import jax.numpy as jnp
from jax import lax
from jax.experimental import pallas as pl
from jax.experimental.pallas import tpu as pltpu
from jax.sharding import PartitionSpec as P

MESH = pl.DeviceIdType.MESH
COLS = 2
PIECES = 8
UNITS = 4
LEAD = 2
CUTS = 8


def normalize(rows, norm_gain):
    xf = rows.astype(jnp.float32)
    scale = lax.rsqrt(jnp.mean(xf * xf, axis=-1, keepdims=True) + 1e-06)
    return (xf * scale * norm_gain[None, :]).astype(jnp.bfloat16)


def sparse_form(tokens, norm_gain, expert_ids, route_weights, gate_weight, up_weight, down_weight):
    tok_rows, half = tokens.shape
    width = half * lax.axis_size("tp")
    experts = lax.axis_size("ep")
    top = expert_ids.shape[1]
    capacity = max(2, (3 * tok_rows * top + 2 * experts - 1) // (2 * experts))
    flat = expert_ids.reshape(-1)
    onehot = (flat[:, None] == jnp.arange(experts, dtype=jnp.int32)[None, :]).astype(jnp.int32)
    earlier = jnp.cumsum(onehot, axis=0) - onehot
    slot = jnp.sum(earlier * onehot, axis=-1)
    position = flat * capacity + slot
    owner = jnp.arange(flat.shape[0], dtype=jnp.int32) // top
    w_gate = gate_weight[0]
    w_up = up_weight[0]
    w_down = down_weight[0]
    send = jnp.zeros((experts * capacity, half), jnp.bfloat16).at[position].set(tokens[owner])
    send = send.reshape(experts, capacity, half)
    received = lax.all_to_all(send, "ep", split_axis=0, concat_axis=0, tiled=True)
    sources = received.shape[0]
    count = received.shape[1]
    whole_rows = lax.all_gather(received, "tp", axis=2, tiled=True)
    rows = normalize(whole_rows.reshape(sources * count, width), norm_gain)
    gate = jnp.dot(rows, w_gate, preferred_element_type=jnp.float32)
    upper = jnp.dot(rows, w_up, preferred_element_type=jnp.float32)
    hidden = (jax.nn.silu(gate) * upper).astype(jnp.bfloat16)
    result = jnp.dot(
        lax.all_gather(hidden, "tp", axis=1, tiled=True), w_down, preferred_element_type=jnp.float32
    )
    result = result.astype(jnp.bfloat16).reshape(sources, count, half)
    back = lax.all_to_all(result, "ep", split_axis=0, concat_axis=0, tiled=True)
    picked = back.reshape(experts * capacity, half)[position].astype(jnp.float32)
    picked = picked * route_weights.reshape(-1)[:, None]
    return jnp.sum(picked.reshape(tok_rows, top, half), axis=1).astype(jnp.bfloat16)


def line_kernel(
    length, cap, tok_ref, gain_in, ids_in, route_in, gate_in, up_in, down_in, out_ref,
    own, gain_ref, ids_ref, route_ref, raw, x, wt, columns, wg, wu, wd, hid, slim_hid, part, came, slim, slim_in, acc,
    swap_s, swap_r, loc, wy_s, wy_r, wx_s, wx_r, gat_s, gat_r, tab_s, tab_r,
    half_s, half_r, hid_s, hid_r, few_s, few_r, sum_s, sum_r, slim_s, slim_r,
):
    f32, bf16 = jnp.float32, jnp.bfloat16
    g, ep, c = lax.axis_index("grp"), lax.axis_index("ep"), lax.axis_index("tp")
    z, y = ep // COLS, ep % COLS
    last = length - 1
    flip = z >= length // 2
    end = jnp.where(flip, last, 0)
    mid = jnp.where(flip, last - 1, 1)
    far_mid, far_end = last - mid, last - end
    outer, inner = z == end, z == mid
    mate, across, beside = {"tp": 1 - c}, {"grp": 1 - g}, {"ep": z * COLS + 1 - y}
    to_end, to_mid, to_far = {"ep": end * COLS + y}, {"ep": mid * COLS + y}, {"ep": far_mid * COLS + y}
    rows, half = raw.shape
    piece = rows // PIECES
    unit = rows // UNITS
    per_unit = PIECES // UNITS
    wide = hid.shape[3]

    def remote(src, dst, ss, rs, dev):
        return pltpu.make_async_remote_copy(
            src_ref=src, dst_ref=dst, send_sem=ss, recv_sem=rs, device_id=dev, device_id_type=MESH
        )

    def span(q):
        return pl.ds(q * piece if isinstance(q, int) else pl.multiple_of(q * piece, piece), piece)

    barrier = pltpu.get_barrier_semaphore()
    for dev in (mate, across, beside):
        pl.semaphore_signal(barrier, inc=1, device_id=dev, device_id_type=MESH)

    @pl.when(outer)
    def _():
        pl.semaphore_signal(barrier, inc=1, device_id=to_mid, device_id_type=MESH)

    @pl.when(inner)
    def _():
        pl.semaphore_signal(barrier, inc=1, device_id=to_end, device_id_type=MESH)
        pl.semaphore_signal(barrier, inc=1, device_id=to_far, device_id_type=MESH)

    inputs = ((tok_ref, own), (gain_in, gain_ref), (ids_in, ids_ref), (route_in, route_ref))
    inputs += ((gate_in, wg.at[0]), (up_in, wu.at[0]), (down_in, wd.at[0]))
    local = [pltpu.make_async_copy(src, dst, loc.at[k]) for k, (src, dst) in enumerate(inputs)]
    for copy in local:
        copy.start()
    pl.semaphore_wait(barrier, jnp.where(outer, 4, 5))

    mats = ((gate_in, wg), (up_in, wu), (down_in, wd))

    def cut(m, portion, u, many=1):
        size = mats[m][0].shape[0] // (2 * CUTS)
        return pl.ds(pl.multiple_of((portion * CUTS + u) * size, size), size * many)

    def send_y(m, u, many=1):
        src, dst = mats[m]
        at = cut(m, g, u, many)
        return remote(src.at[at], dst.at[1, at], wy_s.at[m], wy_r.at[m, u], beside)

    def send_x(m, u, portion, many=1):
        buf = mats[m][1].at[1, cut(m, portion, u, many)]
        return remote(buf, buf, wx_s.at[m], wx_r.at[m], across)

    for m in range(3):
        for u in range(CUTS):
            send_y(m, u).start()

    def swap(q, many=1):
        at = pl.ds(q * piece if isinstance(q, int) else pl.multiple_of(q * piece, piece), piece * many)
        return remote(own.at[at], raw.at[at], swap_s, swap_r.at[q], mate)

    local[0].wait()
    for q in range(PIECES):
        swap(q).start()
    for copy in local[1:4]:
        copy.wait()

    def gather(b, q, way, dev):
        at = x.at[b, c, span(q)]
        return remote(at, at, gat_s.at[way, b], gat_r.at[b, q], dev)

    def gather_sent(b, way, dev):
        remote(x.at[b, c], x.at[b, c], gat_s.at[way, b], gat_r.at[b, 0], dev).wait_send()

    def table(b, way, dev):
        return remote(wt.at[b], wt.at[b], tab_s.at[way, b], tab_r.at[b], dev)

    def share(b, q):
        at = x.at[b, c, span(q)]
        return remote(at, at, half_s.at[b], half_r.at[b, q // per_unit], mate)

    def shared(b, part_of):
        at = x.at[b, 1 - c, rows_of(part_of)]
        remote(at, at, half_s.at[b], half_r.at[b, part_of], mate).wait_recv()

    def rows_of(part_of):
        return pl.ds(part_of * unit if isinstance(part_of, int) else pl.multiple_of(part_of * unit, unit), unit)

    def total(b, q, dev):
        return remote(part.at[b, span(q)], came.at[b, span(q)], sum_s.at[b], sum_r.at[b, q], dev)

    def total_sent(b, dev):
        remote(part.at[b], came.at[b], sum_s.at[b], sum_r.at[b, 0], dev).wait_send()

    def compact(s, dev):
        return remote(slim.at[s], slim_in.at[s], slim_s, slim_r.at[s], dev)

    def hand(pair, s):
        at = hid.at[2 * pair + s, c]
        return remote(at, at, hid_s, hid_r.at[pair], mate)

    def hand_few(s, side):
        at = slim_hid.at[s, side]
        return remote(at, at, few_s, few_r.at[s], mate)

    named = lax.broadcasted_iota(jnp.int32, wt.shape[1:], 0)
    routes = None
    for k in range(ids_ref.shape[0]):
        term = jnp.where(named == ids_ref[pl.ds(k, 1)], route_ref[pl.ds(k, 1)], 0.0)
        routes = term if routes is None else routes + term
    wt[z] = routes

    @pl.when(outer)
    def _():
        table(z, 0, to_mid).start()

    @pl.when(inner)
    def _():
        table(z, 0, to_end).start()
        table(z, 1, to_far).start()

    def norm(q, carry):
        swap(q).wait_recv()
        at = span(q)
        a = own[at].astype(f32)
        b = raw[at].astype(f32)
        total_sq = jnp.sum(a * a, axis=-1, keepdims=True) + jnp.sum(b * b, axis=-1, keepdims=True)
        scale = lax.rsqrt(total_sq / (2 * half) + 1e-06)
        x[z, c, at] = (a * scale * gain_ref[c]).astype(bf16)
        x[z, 1 - c, at] = (b * scale * gain_ref[1 - c]).astype(bf16)

        @pl.when(outer)
        def _():
            gather(z, q, 0, to_mid).start()

        @pl.when(inner)
        def _():
            gather(z, q, 0, to_end).start()

            @pl.when(q < LEAD)
            def _():
                gather(z, q, 1, to_far).start()
        return carry

    lax.fori_loop(0, PIECES, norm, 0)
    columns[z] = wt[z].T

    def got_y(n):
        for m in range(3):
            @pl.when(n // (CUTS // 2) == m)
            def _():
                for v in range(2):
                    u = n % (CUTS // 2) * 2 + v
                    send_y(m, u).wait_recv()
                    send_x(m, u, g).start()

    def got_x(m):
        send_x(m, 0, 1 - g, CUTS).wait_recv()

    def outer_stream(j):
        b = jnp.where(j < PIECES, mid, jnp.where(j < 2 * PIECES, far_end, far_mid))
        q = j % PIECES
        gather(b, q, 0, to_mid).wait_recv()
        share(b, q).start()

    def inner_stream(j):
        lead = j < LEAD
        turn = (j >= LEAD) & (j < LEAD + PIECES)
        b = jnp.where(turn, far_end, far_mid)
        q = jnp.where(lead, j, jnp.where(turn, j - LEAD, j - PIECES))
        gather(b, q, 1, to_far).wait_recv()
        share(b, q).start()

        @pl.when(j >= LEAD)
        def _():
            gather(b, q, 0, to_end).start()

        @pl.when(j == LEAD + PIECES - 1)
        def _():
            for early in range(LEAD):
                gather(far_mid, early, 0, to_end).start()

    def inner_end(q):
        gather(end, q, 0, to_end).wait_recv()
        share(end, q).start()
        gather(end, q, 1, to_far).start()

        @pl.when(q == PIECES - 1)
        def _():
            for late in range(LEAD, PIECES):
                gather(z, late, 1, to_far).start()

    def pick(table_rows, e):
        lane = lax.broadcasted_iota(jnp.int32, table_rows.shape, 0)
        return jnp.sum(jnp.where(lane == e, table_rows, 0.0), axis=0, keepdims=True)

    def selection(b, e):
        weights = wt[b]
        chosen = jnp.where(weights > 0.0, 1.0, 0.0)
        above = lax.broadcasted_iota(jnp.int32, (rows, rows), 0)
        along = lax.broadcasted_iota(jnp.int32, (rows, rows), 1)
        before = jnp.where(above < along, 1.0, 0.0).astype(bf16)
        rank = jnp.dot(chosen.astype(bf16), before, preferred_element_type=f32)
        place = pick(jnp.where(chosen > 0.0, rank, -1.0), e)
        slot = lax.broadcasted_iota(jnp.int32, (cap, rows), 0).astype(f32)
        return jnp.where(slot == place, 1.0, 0.0), pick(weights, e)

    def hidden_half(first, second, s):
        both = []
        for w in (wg, wu):
            both.append(
                jnp.dot(first, w[s, :half], preferred_element_type=f32)
                + jnp.dot(second, w[s, half:], preferred_element_type=f32)
            )
        gate, upper = both
        return (gate * (0.5 * (1.0 + jnp.tanh(0.5 * gate))) * upper).astype(bf16)

    def lowered(left, right, s):
        return jnp.dot(left, wd[s, :wide], preferred_element_type=f32) + jnp.dot(
            right, wd[s, wide:], preferred_element_type=f32
        )

    def slim_rows(s):
        mark, weight_row = selection(mid, end * COLS + (y if s == 0 else 1 - y))
        ones = mark.astype(bf16)
        first = jnp.dot(ones, x[mid, 0], preferred_element_type=f32).astype(bf16)
        second = jnp.dot(ones, x[mid, 1], preferred_element_type=f32).astype(bf16)
        slim_hid[s, c] = hidden_half(first, second, s)
        hand_few(s, c).start()
        weight = jnp.sum(mark * weight_row, axis=1, keepdims=True)
        hand_few(s, 1 - c).wait_recv()
        slim[s] = (lowered(slim_hid[s, 0], slim_hid[s, 1], s) * weight).astype(bf16)

    def widen(s):
        mark, _ = selection(mid, end * COLS + (y if s == 0 else 1 - y))
        ones = mark.astype(bf16)
        return lax.dot_general(ones, slim_in[s], (((0,), (0,)), ((), ())), preferred_element_type=f32)

    def block_of(k):
        return jnp.where(k == 0, far_end, jnp.where(k == 1, end, jnp.where(k == 2, far_mid, mid)))

    def first_stage(code):
        pair, s = code // 2, code % 2
        b, part_of = block_of(pair // UNITS), pair % UNITS

        @pl.when((s == 0) & (b != z))
        def _():
            shared(b, part_of)

        at = rows_of(part_of)
        hid[code, c] = hidden_half(x[b, 0, at], x[b, 1, at], s)
        hand(pair, s).start()

    def second_stage(pair):
        b, part_of = block_of(pair // UNITS), pair % UNITS
        at = rows_of(part_of)
        mine = columns[b, at]
        lane = lax.broadcasted_iota(jnp.int32, mine.shape, 1)
        both = hid.at[pl.ds(2 * pair, 2), 1 - c]
        remote(both, both, hid_s, hid_r.at[pair], mate).wait_recv()
        sums = None
        for s in range(2):
            expert = z * COLS + (y if s == 0 else 1 - y)
            weight = jnp.sum(jnp.where(lane == expert, mine, 0.0), axis=1, keepdims=True)
            got = lowered(hid[2 * pair + s, 0], hid[2 * pair + s, 1], s) * weight
            sums = got if sums is None else sums + got

        @pl.when(b == z)
        def _():
            acc[at] = sums

        @pl.when(b != z)
        def _():
            part[b, at] = sums.astype(bf16)

        @pl.when(outer & (b != z))
        def _():
            for n in range(per_unit):
                total(b, part_of * per_unit + n, to_mid).start()

    def pass_on(b, q, dev):
        total(b, q, dev).wait_recv()
        at = span(q)
        part[b, at] = (part[b, at].astype(f32) + came[b, at].astype(f32)).astype(bf16)
        total(b, q, dev).start()

    def take_in(q):
        total(z, q, to_far).wait_recv()
        at = span(q)
        acc[at] = acc[at] + came[z, at].astype(f32)

    def look(n, entries):
        value = 0
        for at, entry in entries.items():
            value = jnp.where(n == at, entry, value)
        return value

    head = 3 * CUTS // 2
    outer_first = {
        0: ((1, 0, 0), (1, 1, 0)), 1: ((1, 2, 0), (1, 3, 0)), 11: ((0, 0, 0), (0, 0, 1)), 12: ((0, 1, 0), (0, 1, 1)),
        13: ((1, 0, 1), (1, 1, 1)), 14: ((0, 2, 0), (0, 2, 1)), 15: ((1, 2, 1), (1, 3, 1)), 17: ((0, 3, 0), (0, 3, 1)),
        19: ((2, 0, 0), (2, 0, 1)), 21: ((2, 1, 0), (2, 1, 1)), 23: ((2, 2, 0), (2, 2, 1)), 25: ((2, 3, 0), (2, 3, 1)),
    }
    outer_second = {
        11: ((0, 0),), 12: ((0, 1),), 14: ((0, 2),), 16: ((1, 0), (1, 1)), 17: ((0, 3),), 18: ((1, 2), (1, 3)),
        19: ((2, 0),), 21: ((2, 1),), 23: ((2, 2),), 25: ((2, 3),),
    }
    outer_pairs = {13: 13, 16: 15, 18: 17, 20: 19, 22: 21, 24: 23}
    inner_first = {
        0: ((3, 0, 0), (3, 1, 0)), 1: ((3, 2, 0), (3, 3, 0)), 2: ((1, 0, 0),), 3: ((2, 0, 0),),
        4: ((1, 1, 0), (0, 0, 0)), 6: ((1, 2, 0), (0, 1, 0)), 8: ((1, 3, 0), (0, 2, 0)),
        9: ((0, 0, 1), (0, 1, 1)), 11: ((0, 3, 0), (0, 2, 1), (0, 3, 1)),
        14: ((1, 0, 1), (1, 1, 1)), 15: ((1, 2, 1), (1, 3, 1)), 16: ((2, 0, 1), (2, 1, 0)), 17: ((2, 1, 1), (2, 2, 0)),
        18: ((2, 2, 1), (2, 3, 0)), 19: ((2, 3, 1), (3, 0, 1)), 20: ((3, 1, 1), (3, 2, 1)), 21: ((3, 3, 1),),
    }
    inner_second = {
        12: ((0, 0), (0, 1)), 13: ((0, 2), (0, 3)), 15: ((1, 0), (1, 1)), 16: ((1, 2), (1, 3)), 17: ((2, 0),),
        18: ((2, 1),), 19: ((2, 2),), 20: ((2, 3), (3, 0)), 21: ((3, 1), (3, 2)), 22: ((3, 3),),
    }

    def packed(plan, width):
        entries = {}
        for at, todo in plan.items():
            entries[at] = 0
            for k, (blk, part_of, *s) in enumerate(todo):
                number = blk * UNITS + part_of
                entries[at] += ((2 * number + s[0] if s else number) + 1) * width ** k
        return entries

    first_width, second_width = 8 * UNITS * 2, 8 * UNITS
    plans = (
        packed(outer_first, first_width), packed(inner_first, first_width),
        packed(outer_second, second_width), packed(inner_second, second_width),
    )

    for copy in local[4:]:
        copy.wait()

    @pl.when(outer)
    def _():
        table(mid, 0, to_mid).wait_recv()

    @pl.when(inner)
    def _():
        table(end, 0, to_end).wait_recv()
        table(end, 1, to_far).start()
        table(far_mid, 1, to_far).wait_recv()
        table(far_mid, 0, to_end).start()
        for b in (end, far_mid):
            columns[b] = wt[b].T

    def step(n, carry):
        @pl.when(n < head)
        def _():
            got_y(n)

        ahead = look(n, outer_pairs)

        @pl.when(outer)
        def _():
            @pl.when(n == PIECES)
            def _():
                for u in range(UNITS):
                    shared(mid, u)
                slim_rows(0)
                compact(0, to_mid).start()

            @pl.when(n < head)
            def _():
                outer_stream(n)

            @pl.when(ahead > 0)
            def _():
                outer_stream(ahead - 1)
                outer_stream(ahead)

        @pl.when(inner)
        def _():
            @pl.when(n < PIECES)
            def _():
                inner_end(n)

            @pl.when((n < head) | ((n >= head + 2) & (n < head + 6)))
            def _():
                inner_stream(jnp.where(n < head, n, n - 2))

            @pl.when(n == LEAD)
            def _():
                table(far_end, 1, to_far).wait_recv()
                table(far_end, 0, to_end).start()
                columns[far_end] = wt[far_end].T

        @pl.when(n == PIECES + 1)
        def _():
            got_x(0)
            got_x(1)

        @pl.when(outer)
        def _():
            @pl.when(n == head - 1)
            def _():
                table(far_end, 0, to_mid).wait_recv()
                table(far_mid, 0, to_mid).wait_recv()
                for b in (far_end, far_mid):
                    columns[b] = wt[b].T

        @pl.when(inner)
        def _():
            q = n - head - 2

            @pl.when((q >= 0) & (q < PIECES))
            def _():
                pass_on(far_end, q, to_far)

            @pl.when((q >= 3) & (q < PIECES + 3))
            def _():
                pass_on(end, q - 3, to_end)

            @pl.when((q >= PIECES) & (q < 2 * PIECES))
            def _():
                pass_on(far_mid, q - PIECES, to_far)

            @pl.when(q == PIECES + 1)
            def _():
                compact(0, to_end).wait_recv()
                acc[...] = acc[...] + widen(0)

            @pl.when(q >= PIECES + 2)
            def _():
                take_in(q - PIECES - 2)

        todo = jnp.where(outer, look(n, plans[0]), look(n, plans[1]))

        def first(v, left):
            code = left % first_width

            @pl.when(code > 0)
            def _():
                first_stage(code - 1)
            return left // first_width

        lax.fori_loop(0, 4, first, todo)

        @pl.when(n == jnp.where(outer, head - 1, head))
        def _():
            got_x(2)

        todo = jnp.where(outer, look(n, plans[2]), look(n, plans[3]))

        def second(v, left):
            pair = left % second_width

            @pl.when(pair > 0)
            def _():
                second_stage(pair - 1)
            return left // second_width

        lax.fori_loop(0, 2, second, todo)

        @pl.when(outer & (n == head + 3))
        def _():
            slim_rows(1)
        return carry

    lax.fori_loop(0, 4 * PIECES, step, 0)

    @pl.when(outer)
    def _():
        compact(1, to_mid).start()

    @pl.when(outer)
    def _():
        for q in range(PIECES):
            total(z, q, to_mid).wait_recv()
            at = span(q)
            out_ref[at] = (acc[at] + came[z, at].astype(f32)).astype(bf16)

    @pl.when(inner)
    def _():
        compact(1, to_end).wait_recv()
        out_ref[...] = (acc[...] + widen(1)).astype(bf16)

    swap(0, PIECES).wait_send()
    for m in range(3):
        send_y(m, 0, CUTS).wait_send()
        send_x(m, 0, g, CUTS).wait_send()

    def handed(count):
        at = hid.at[pl.ds(0, count), c]
        remote(at, at, hid_s, hid_r.at[0], mate).wait_send()

    def blocks_shared(blocks):
        for b in blocks:
            remote(x.at[b, c], x.at[b, c], half_s.at[b], half_r.at[b, 0], mate).wait_send()

    @pl.when(outer)
    def _():
        table(z, 0, to_mid).wait_send()
        remote(slim, slim_in, slim_s, slim_r.at[0], to_mid).wait_send()
        at = slim_hid.at[pl.ds(0, 2), c]
        remote(at, at, few_s, few_r.at[0], mate).wait_send()
        handed(6 * UNITS)
        gather_sent(z, 0, to_mid)
        for b in (far_end, far_mid):
            total_sent(b, to_mid)
        blocks_shared((mid, far_end, far_mid))

    @pl.when(inner)
    def _():
        handed(8 * UNITS)
        table(z, 0, to_end).wait_send()
        table(z, 1, to_far).wait_send()
        table(end, 1, to_far).wait_send()
        table(far_mid, 0, to_end).wait_send()
        table(far_end, 0, to_end).wait_send()
        for b in (z, far_mid, far_end):
            gather_sent(b, 0, to_end)
        for b in (z, end):
            gather_sent(b, 1, to_far)
        total_sent(end, to_end)
        for b in (far_mid, far_end):
            total_sent(b, to_far)
        blocks_shared((end, far_mid, far_end))


def line_form(tokens, norm_gain, expert_ids, route_weights, gate_weight, up_weight, down_weight):
    tok_rows, half = tokens.shape
    experts = lax.axis_size("ep")
    length = experts // COLS
    top = expert_ids.shape[1]
    cap = (3 * tok_rows * top + 2 * experts - 1) // (2 * experts)
    bf16, f32 = jnp.bfloat16, jnp.float32
    gate, up, down = gate_weight[0], up_weight[0], down_weight[0]
    dma, vmem = pltpu.SemaphoreType.DMA, pltpu.VMEM
    block = (length, tok_rows, half)
    pairs = UNITS * length
    bits = (length, PIECES)
    sems = [dma, dma((PIECES,)), dma((7,))]
    for send, recv in (
        ((3,), (3, CUTS)), ((3,), (3,)), ((2, length), bits), ((2, length), (length,)),
        ((length,), (length, UNITS)), ((), (pairs,)), ((), (2,)), ((length,), bits), ((), (2,)),
    ):
        sems += [dma(send) if send else dma, dma(recv)]
    return pl.pallas_call(
        functools.partial(line_kernel, length, cap),
        out_shape=vmem((tok_rows, half), bf16),
        in_specs=[pl.BlockSpec(memory_space=pl.ANY)] * 7,
        out_specs=pl.BlockSpec(memory_space=vmem),
        scratch_shapes=[
            vmem((tok_rows, half), bf16),
            vmem((2, 1, half), f32),
            vmem((top, tok_rows), jnp.int32),
            vmem((top, tok_rows), f32),
            vmem((tok_rows, half), bf16),
            vmem((length, 2, tok_rows, half), bf16),
            vmem((length, experts, tok_rows), f32),
            vmem((length, tok_rows, experts), f32),
            vmem((2,) + gate.shape, bf16),
            vmem((2,) + up.shape, bf16),
            vmem((2,) + down.shape, bf16),
            vmem((2 * pairs, 2, tok_rows // UNITS, gate.shape[1]), bf16),
            vmem((2, 2, cap, gate.shape[1]), bf16),
            vmem(block, bf16),
            vmem(block, bf16),
            vmem((2, cap, half), bf16),
            vmem((2, cap, half), bf16),
            vmem((tok_rows, half), f32),
        ]
        + sems,
        compiler_params=pltpu.CompilerParams(
            collective_id=0, has_side_effects=True, vmem_limit_bytes=58 * 1024 * 1024
        ),
    )(tokens, norm_gain.reshape(2, 1, half), expert_ids.T, route_weights.T, gate, up, down)


def solution(mesh):
    in_specs = (
        P(("grp", "ep"), "tp"),
        P(),
        P(("grp", "ep"), None),
        P(("grp", "ep"), None),
        P("ep", None, "tp"),
        P("ep", None, "tp"),
        P("ep", None, "tp"),
    )
    out_specs = P(("grp", "ep"), "tp")
    shape = mesh.shape

    def on_device(tokens, norm_gain, expert_ids, *rest):
        dense = shape["ep"] == 4 * COLS and shape["ep"] == 4 * expert_ids.shape[1]
        form = line_form if dense and shape["grp"] == 2 and shape["tp"] == 2 else sparse_form
        return form(tokens, norm_gain, expert_ids, *rest)

    return jax.shard_map(
        on_device, mesh=mesh, in_specs=in_specs, out_specs=out_specs, check_vma=False
    )
```

time: 117 us -> 102 us (0.87)
  Pallas kernels: 112 us -> 101 us
  local copies, waits for them, and re-layouts: 2.95 us -> 0.97 us
  other arithmetic: 1.3 us -> 0 us
    pallas_call x1, Pallas kernels: 112 us -> 101 us  [line_form(): pl.pallas_call(functools.partial(line_kernel, length, cap), out_shape=vme...]
    unnamed x3 -> x1, local copies, waits for them, and re-layouts: 2.95 us -> 0.97 us
    reduce_sum x1 -> x0, other arithmetic: 1.3 us -> none  [line_form(): route = jnp.sum(jnp.where(chosen, route_weights[None], 0.0), axis=-1)]
where the time goes in v2:
time: 102 us
  Pallas kernels  101 us (99%)
    pallas_call x1, Pallas kernels, line_form(): pl.pallas_call(functools.partial(line_kernel, length, cap), out_shape=vme...  101 us

profile of v2, /device:TPU:8, one launch (start us, length us, event | category | flops | bytes accessed | tf_op | source)
XLA Modules:
  0.0 101.9 jit_solution(10564034041448399870)
XLA Ops:
  0.0 101.0 %shard_map.73 = bf16[512,1024]{1,0:T(8,128)(2,1)S(1)} custom-call(bf16[512,1024]{1,0:T(8,128)(2,1)} %tok_ref.1, f32[2,1,1024]{2,1,0:T(1,128)} %bitcast.9, s32[2,512]{1,0:T(2,128)} %bitcast.10, f32[2,512]{1,0:T(2,128)} %bitcast.11, bf16[2048,256]{1,0:T(8,128)(2,1)} %bitcast.6, bf16[2048,256]{1,0:T(8,128)(2,1)} %bitcast.7, bf16[512,1024]{1,0:T(8,128)(2,1)} %bitcast.8), custom_call_target="tpu_custom_call" | custom-call | tf_op jit(solution)/shard_map/pallas_call | solution.py:615
  101.0 1.0 copy.9

commit v3 on v2

--- a/solution.py
+++ b/solution.py
@@ -58,9 +58,9 @@
 
 def line_kernel(
     length, cap, tok_ref, gain_in, ids_in, route_in, gate_in, up_in, down_in, out_ref,
-    own, gain_ref, ids_ref, route_ref, raw, x, wt, columns, wg, wu, wd, hid, slim_hid, part, came, slim, slim_in, acc,
+    own, gain_ref, ids_ref, route_ref, raw, x, wt, columns, wg, wu, wd, hid, slim_hid, picked, slim_w, part, came, slim, slim_in, acc,
     swap_s, swap_r, loc, wy_s, wy_r, wx_s, wx_r, gat_s, gat_r, tab_s, tab_r,
-    half_s, half_r, hid_s, hid_r, few_s, few_r, sum_s, sum_r, slim_s, slim_r,
+    half_s, half_r, hid_s, hid_r, few_s, few_r, pick_s, pick_r, match_s, match_r, sum_s, sum_r, slim_s, slim_r,
 ):
     f32, bf16 = jnp.float32, jnp.bfloat16
     g, ep, c = lax.axis_index("grp"), lax.axis_index("ep"), lax.axis_index("tp")
@@ -109,18 +109,25 @@
 
     mats = ((gate_in, wg), (up_in, wu), (down_in, wd))
 
+    columns_cut = down_in.shape[1] // CUTS
+
     def cut(m, portion, u, many=1):
-        size = mats[m][0].shape[0] // (2 * CUTS)
-        return pl.ds(pl.multiple_of((portion * CUTS + u) * size, size), size * many)
+        if m < 2:
+            size = mats[m][0].shape[0] // (2 * CUTS)
+            return (pl.ds(pl.multiple_of((portion * CUTS + u) * size, size), size * many), pl.ds(0, wide))
+        first = pl.multiple_of((portion * (CUTS // 2) + u // 2) * columns_cut, columns_cut)
+        if many == 1:
+            return (pl.ds(pl.multiple_of(u % 2 * wide, wide), wide), pl.ds(first, columns_cut))
+        return (pl.ds(0, 2 * wide), pl.ds(first, columns_cut * (many // 2)))
 
     def send_y(m, u, many=1):
         src, dst = mats[m]
         at = cut(m, g, u, many)
-        return remote(src.at[at], dst.at[1, at], wy_s.at[m], wy_r.at[m, u], beside)
+        return remote(src.at[at], dst.at[(1,) + at], wy_s.at[m], wy_r.at[m, u], beside)
 
     def send_x(m, u, portion, many=1):
-        buf = mats[m][1].at[1, cut(m, portion, u, many)]
-        return remote(buf, buf, wx_s.at[m], wx_r.at[m], across)
+        buf = mats[m][1].at[(1,) + cut(m, portion, u, many)]
+        return remote(buf, buf, wx_s.at[m], wx_r.at[m if m < 2 else 2 + u // 2], across)
 
     for m in range(3):
         for u in range(CUTS):
@@ -169,6 +176,17 @@
     def hand(pair, s):
         at = hid.at[2 * pair + s, c]
         return remote(at, at, hid_s, hid_r.at[pair], mate)
+
+    def chosen_rows(s, dev):
+        at = picked.at[s, c]
+        return remote(at, at, pick_s, pick_r.at[s], dev)
+
+    def match(s, side):
+        at = picked.at[s, side]
+        return remote(at, at, match_s, match_r.at[s], mate)
+
+    def compact_columns(at):
+        return remote(slim.at[1, :, at], slim_in.at[1, :, at], slim_s, slim_r.at[1], to_mid)
 
     def hand_few(s, side):
         at = slim_hid.at[s, side]
@@ -206,8 +224,6 @@
 
         @pl.when(inner)
         def _():
-            gather(z, q, 0, to_end).start()
-
             @pl.when(q < LEAD)
             def _():
                 gather(z, q, 1, to_far).start()
@@ -228,8 +244,11 @@
     def got_x(m):
         send_x(m, 0, 1 - g, CUTS).wait_recv()
 
+    def got_columns(k):
+        send_x(2, 2 * k, 1 - g, 2).wait_recv()
+
     def outer_stream(j):
-        b = jnp.where(j < PIECES, mid, jnp.where(j < 2 * PIECES, far_end, far_mid))
+        b = jnp.where(j < PIECES, far_end, far_mid)
         q = j % PIECES
         gather(b, q, 0, to_mid).wait_recv()
         share(b, q).start()
@@ -291,16 +310,45 @@
             right, wd[s, wide:], preferred_element_type=f32
         )
 
-    def slim_rows(s):
+    def pick_rows(s):
+        mark, _ = selection(mid, end * COLS + (y if s == 0 else 1 - y))
+        picked[s, c] = jnp.dot(mark.astype(bf16), x[mid, c], preferred_element_type=f32).astype(bf16)
+        chosen_rows(s, to_end).start()
+
+    def got_rows(s):
+        chosen_rows(s, to_mid).wait_recv()
+        match(s, c).start()
+
+    def slim_first(s):
+        match(s, 1 - c).wait_recv()
+        slim_hid[s, c] = hidden_half(picked[s, 0], picked[s, 1], s)
+        hand_few(s, c).start()
+
+    def slim_weight(s):
         mark, weight_row = selection(mid, end * COLS + (y if s == 0 else 1 - y))
-        ones = mark.astype(bf16)
-        first = jnp.dot(ones, x[mid, 0], preferred_element_type=f32).astype(bf16)
-        second = jnp.dot(ones, x[mid, 1], preferred_element_type=f32).astype(bf16)
-        slim_hid[s, c] = hidden_half(first, second, s)
-        hand_few(s, c).start()
-        weight = jnp.sum(mark * weight_row, axis=1, keepdims=True)
-        hand_few(s, 1 - c).wait_recv()
-        slim[s] = (lowered(slim_hid[s, 0], slim_hid[s, 1], s) * weight).astype(bf16)
+        return jnp.sum(mark * weight_row, axis=1, keepdims=True)
+
+    def slim_rows():
+        slim_first(0)
+        weight = slim_weight(0)
+        hand_few(0, 1 - c).wait_recv()
+        slim[0] = (lowered(slim_hid[0, 0], slim_hid[0, 1], 0) * weight).astype(bf16)
+        compact(0, to_mid).start()
+
+    def columns_at(k, portion):
+        return pl.ds(pl.multiple_of((portion * (CUTS // 2) + k) * columns_cut, columns_cut), columns_cut)
+
+    def slim_columns(k):
+        for portion in (g, 1 - g):
+            at = columns_at(k, portion)
+            got = jnp.dot(slim_hid[1, 0], wd[1, :wide, at], preferred_element_type=f32) + jnp.dot(
+                slim_hid[1, 1], wd[1, wide:, at], preferred_element_type=f32
+            )
+            slim[1, :, at] = (got * slim_w[...]).astype(bf16)
+
+    def send_columns(k):
+        for portion in (g, 1 - g):
+            compact_columns(columns_at(k, portion)).start()
 
     def widen(s):
         mark, _ = selection(mid, end * COLS + (y if s == 0 else 1 - y))
@@ -368,15 +416,15 @@
 
     head = 3 * CUTS // 2
     outer_first = {
-        0: ((1, 0, 0), (1, 1, 0)), 1: ((1, 2, 0), (1, 3, 0)), 11: ((0, 0, 0), (0, 0, 1)), 12: ((0, 1, 0), (0, 1, 1)),
-        13: ((1, 0, 1), (1, 1, 1)), 14: ((0, 2, 0), (0, 2, 1)), 15: ((1, 2, 1), (1, 3, 1)), 17: ((0, 3, 0), (0, 3, 1)),
+        0: ((1, 0, 0), (1, 1, 0)), 1: ((1, 2, 0), (1, 3, 0)), 10: ((0, 0, 0), (0, 0, 1)), 11: ((0, 1, 0), (0, 1, 1)),
+        13: ((0, 2, 0), (0, 2, 1)), 14: ((1, 0, 1), (1, 1, 1)), 15: ((0, 3, 0), (0, 3, 1)), 16: ((1, 2, 1), (1, 3, 1)),
         19: ((2, 0, 0), (2, 0, 1)), 21: ((2, 1, 0), (2, 1, 1)), 23: ((2, 2, 0), (2, 2, 1)), 25: ((2, 3, 0), (2, 3, 1)),
     }
     outer_second = {
-        11: ((0, 0),), 12: ((0, 1),), 14: ((0, 2),), 16: ((1, 0), (1, 1)), 17: ((0, 3),), 18: ((1, 2), (1, 3)),
+        12: ((0, 0), (0, 1)), 13: ((0, 2),), 15: ((0, 3),), 16: ((1, 0), (1, 1)), 17: ((1, 2), (1, 3)),
         19: ((2, 0),), 21: ((2, 1),), 23: ((2, 2),), 25: ((2, 3),),
     }
-    outer_pairs = {13: 13, 16: 15, 18: 17, 20: 19, 22: 21, 24: 23}
+    outer_pairs = {13: 5, 15: 7, 18: 9, 20: 11, 22: 13, 24: 15}
     inner_first = {
         0: ((3, 0, 0), (3, 1, 0)), 1: ((3, 2, 0), (3, 3, 0)), 2: ((1, 0, 0),), 3: ((2, 0, 0),),
         4: ((1, 1, 0), (0, 0, 0)), 6: ((1, 2, 0), (0, 1, 0)), 8: ((1, 3, 0), (0, 2, 0)),
@@ -413,6 +461,8 @@
 
     @pl.when(inner)
     def _():
+        for s in range(2):
+            pick_rows(s)
         table(end, 0, to_end).wait_recv()
         table(end, 1, to_far).start()
         table(far_mid, 1, to_far).wait_recv()
@@ -429,16 +479,19 @@
 
         @pl.when(outer)
         def _():
-            @pl.when(n == PIECES)
-            def _():
-                for u in range(UNITS):
-                    shared(mid, u)
-                slim_rows(0)
-                compact(0, to_mid).start()
-
-            @pl.when(n < head)
-            def _():
-                outer_stream(n)
+            @pl.when(n == PIECES // 2)
+            def _():
+                got_rows(0)
+                slim_rows()
+
+            @pl.when(n == PIECES - 1)
+            def _():
+                got_rows(1)
+                slim_w[...] = jnp.broadcast_to(slim_weight(1), slim_w.shape)
+
+            @pl.when((n >= PIECES) & (n < head))
+            def _():
+                outer_stream(n - PIECES)
 
             @pl.when(ahead > 0)
             def _():
@@ -465,6 +518,26 @@
         def _():
             got_x(0)
             got_x(1)
+
+        @pl.when(outer)
+        def _():
+            @pl.when(n == PIECES + 1)
+            def _():
+                slim_first(1)
+
+            for k in range(CUTS // 2):
+                @pl.when(n == min(head, PIECES + 2 + k))
+                def _():
+                    got_columns(k)
+                    if k == 0:
+                        hand_few(1, 1 - c).wait_recv()
+                    if k < CUTS // 2 - 1:
+                        slim_columns(k)
+                        send_columns(k)
+
+            @pl.when(n == head + 2)
+            def _():
+                slim_columns(CUTS // 2 - 1)
 
         @pl.when(outer)
         def _():
@@ -496,6 +569,11 @@
                 compact(0, to_end).wait_recv()
                 acc[...] = acc[...] + widen(0)
 
+            @pl.when(n == 4 * PIECES - 1)
+            def _():
+                compact(1, to_end).wait_recv()
+                acc[...] = acc[...] + widen(1)
+
             @pl.when(q >= PIECES + 2)
             def _():
                 take_in(q - PIECES - 2)
@@ -512,9 +590,10 @@
 
         lax.fori_loop(0, 4, first, todo)
 
-        @pl.when(n == jnp.where(outer, head - 1, head))
-        def _():
-            got_x(2)
+        @pl.when(inner & (n == head))
+        def _():
+            for k in range(CUTS // 2):
+                got_columns(k)
 
         todo = jnp.where(outer, look(n, plans[2]), look(n, plans[3]))
 
@@ -528,16 +607,12 @@
 
         lax.fori_loop(0, 2, second, todo)
 
-        @pl.when(outer & (n == head + 3))
-        def _():
-            slim_rows(1)
+        @pl.when(outer & (n == 3 * PIECES + 2))
+        def _():
+            send_columns(CUTS // 2 - 1)
         return carry
 
     lax.fori_loop(0, 4 * PIECES, step, 0)
-
-    @pl.when(outer)
-    def _():
-        compact(1, to_mid).start()
 
     @pl.when(outer)
     def _():
@@ -548,8 +623,7 @@
 
     @pl.when(inner)
     def _():
-        compact(1, to_end).wait_recv()
-        out_ref[...] = (acc[...] + widen(1)).astype(bf16)
+        out_ref[...] = acc[...].astype(bf16)
 
     swap(0, PIECES).wait_send()
     for m in range(3):
@@ -571,10 +645,12 @@
         at = slim_hid.at[pl.ds(0, 2), c]
         remote(at, at, few_s, few_r.at[0], mate).wait_send()
         handed(6 * UNITS)
+        at = picked.at[pl.ds(0, 2), c]
+        remote(at, at, match_s, match_r.at[0], mate).wait_send()
         gather_sent(z, 0, to_mid)
         for b in (far_end, far_mid):
             total_sent(b, to_mid)
-        blocks_shared((mid, far_end, far_mid))
+        blocks_shared((far_end, far_mid))
 
     @pl.when(inner)
     def _():
@@ -584,7 +660,9 @@
         table(end, 1, to_far).wait_send()
         table(far_mid, 0, to_end).wait_send()
         table(far_end, 0, to_end).wait_send()
-        for b in (z, far_mid, far_end):
+        at = picked.at[pl.ds(0, 2), c]
+        remote(at, at, pick_s, pick_r.at[0], to_end).wait_send()
+        for b in (far_mid, far_end):
             gather_sent(b, 0, to_end)
         for b in (z, end):
             gather_sent(b, 1, to_far)
@@ -608,8 +686,8 @@
     bits = (length, PIECES)
     sems = [dma, dma((PIECES,)), dma((7,))]
     for send, recv in (
-        ((3,), (3, CUTS)), ((3,), (3,)), ((2, length), bits), ((2, length), (length,)),
-        ((length,), (length, UNITS)), ((), (pairs,)), ((), (2,)), ((length,), bits), ((), (2,)),
+        ((3,), (3, CUTS)), ((3,), (2 + CUTS // 2,)), ((2, length), bits), ((2, length), (length,)),
+        ((length,), (length, UNITS)), ((), (pairs,)), ((), (2,)), ((), (2,)), ((), (2,)), ((length,), bits), ((), (2,)),
     ):
         sems += [dma(send) if send else dma, dma(recv)]
     return pl.pallas_call(
@@ -631,6 +709,8 @@
             vmem((2,) + down.shape, bf16),
             vmem((2 * pairs, 2, tok_rows // UNITS, gate.shape[1]), bf16),
             vmem((2, 2, cap, gate.shape[1]), bf16),
+            vmem((2, 2, cap, half), bf16),
+            vmem((cap, half // CUTS), f32),
             vmem(block, bf16),
             vmem(block, bf16),
             vmem((2, cap, half), bf16),

time: 102 us -> 99.6 us (0.976)
  Pallas kernels: 101 us -> 98.5 us
    pallas_call x1, Pallas kernels: 101 us -> 98.5 us  [line_form(): pl.pallas_call(functools.partial(line_kernel, length, cap), out_shape=vme...]
where the time goes in v3:
time: 99.6 us; the launch traced here: 99.5 us
  Pallas kernels  98.5 us (99%)
    pallas_call x1, Pallas kernels, line_form(): pl.pallas_call(functools.partial(line_kernel, length, cap), out_shape=vme...  98.5 us

profile of v3, /device:TPU:8, one launch (start us, length us, event | category | flops | bytes accessed | tf_op | source)
XLA Modules:
  0.0 99.5 jit_solution(17141509626445064812)
XLA Ops:
  0.0 98.5 %shard_map.73 = bf16[512,1024]{1,0:T(8,128)(2,1)S(1)} custom-call(bf16[512,1024]{1,0:T(8,128)(2,1)} %tok_ref.1, f32[2,1,1024]{2,1,0:T(1,128)} %bitcast.9, s32[2,512]{1,0:T(2,128)} %bitcast.10, f32[2,512]{1,0:T(2,128)} %bitcast.11, bf16[2048,256]{1,0:T(8,128)(2,1)} %bitcast.6, bf16[2048,256]{1,0:T(8,128)(2,1)} %bitcast.7, bf16[512,1024]{1,0:T(8,128)(2,1)} %bitcast.8), custom_call_target="tpu_custom_call" | custom-call | tf_op jit(solution)/shard_map/pallas_call | solution.py:693
  98.5 1.0 copy.9

commit v4 on v3

--- a/solution.py
+++ b/solution.py
@@ -12,6 +12,7 @@
 PIECES = 8
 UNITS = 4
 LEAD = 2
+SPLIT = 2
 CUTS = 8
 
 
@@ -58,7 +59,7 @@
 
 def line_kernel(
     length, cap, tok_ref, gain_in, ids_in, route_in, gate_in, up_in, down_in, out_ref,
-    own, gain_ref, ids_ref, route_ref, raw, x, wt, columns, wg, wu, wd, hid, slim_hid, picked, slim_w, part, came, slim, slim_in, acc,
+    own, gain_ref, ids_ref, route_ref, raw, x, xn, wt, columns, wg, wu, wd, hid, slim_hid, picked, slim_w, part, came, slim, slim_in, acc,
     swap_s, swap_r, loc, wy_s, wy_r, wx_s, wx_r, gat_s, gat_r, tab_s, tab_r,
     half_s, half_r, hid_s, hid_r, few_s, few_r, pick_s, pick_r, match_s, match_r, sum_s, sum_r, slim_s, slim_r,
 ):
@@ -121,76 +122,32 @@
         return (pl.ds(0, 2 * wide), pl.ds(first, columns_cut * (many // 2)))
 
     def send_y(m, u, many=1):
-        src, dst = mats[m]
+        dst = mats[m][1]
         at = cut(m, g, u, many)
-        return remote(src.at[at], dst.at[(1,) + at], wy_s.at[m], wy_r.at[m, u], beside)
+        return remote(dst.at[(0,) + at], dst.at[(1,) + at], wy_s.at[m], wy_r.at[m, u], beside)
+
+    def send_extra():
+        at = cut(2, 1 - g, CUTS - 2, 2)
+        return remote(
+            wd.at[(0,) + at], wd.at[(1,) + at], wy_s.at[3], wx_r.at[1 + CUTS // 2], beside
+        )
 
     def send_x(m, u, portion, many=1):
         buf = mats[m][1].at[(1,) + cut(m, portion, u, many)]
         return remote(buf, buf, wx_s.at[m], wx_r.at[m if m < 2 else 2 + u // 2], across)
 
-    for m in range(3):
-        for u in range(CUTS):
-            send_y(m, u).start()
-
     def swap(q, many=1):
         at = pl.ds(q * piece if isinstance(q, int) else pl.multiple_of(q * piece, piece), piece * many)
         return remote(own.at[at], raw.at[at], swap_s, swap_r.at[q], mate)
 
-    local[0].wait()
-    for q in range(PIECES):
-        swap(q).start()
-    for copy in local[1:4]:
+    def gather(b, q, way, dev, src=None):
+        at = x.at[b, c, span(q)]
+        return remote(at if src is None else src.at[span(q)], at, gat_s.at[way, b], gat_r.at[b, q], dev)
+
+    for copy in local[2:4]:
         copy.wait()
-
-    def gather(b, q, way, dev):
-        at = x.at[b, c, span(q)]
-        return remote(at, at, gat_s.at[way, b], gat_r.at[b, q], dev)
-
-    def gather_sent(b, way, dev):
-        remote(x.at[b, c], x.at[b, c], gat_s.at[way, b], gat_r.at[b, 0], dev).wait_send()
-
     def table(b, way, dev):
         return remote(wt.at[b], wt.at[b], tab_s.at[way, b], tab_r.at[b], dev)
-
-    def share(b, q):
-        at = x.at[b, c, span(q)]
-        return remote(at, at, half_s.at[b], half_r.at[b, q // per_unit], mate)
-
-    def shared(b, part_of):
-        at = x.at[b, 1 - c, rows_of(part_of)]
-        remote(at, at, half_s.at[b], half_r.at[b, part_of], mate).wait_recv()
-
-    def rows_of(part_of):
-        return pl.ds(part_of * unit if isinstance(part_of, int) else pl.multiple_of(part_of * unit, unit), unit)
-
-    def total(b, q, dev):
-        return remote(part.at[b, span(q)], came.at[b, span(q)], sum_s.at[b], sum_r.at[b, q], dev)
-
-    def total_sent(b, dev):
-        remote(part.at[b], came.at[b], sum_s.at[b], sum_r.at[b, 0], dev).wait_send()
-
-    def compact(s, dev):
-        return remote(slim.at[s], slim_in.at[s], slim_s, slim_r.at[s], dev)
-
-    def hand(pair, s):
-        at = hid.at[2 * pair + s, c]
-        return remote(at, at, hid_s, hid_r.at[pair], mate)
-
-    def chosen_rows(s, dev):
-        at = picked.at[s, c]
-        return remote(at, at, pick_s, pick_r.at[s], dev)
-
-    def match(s, side):
-        at = picked.at[s, side]
-        return remote(at, at, match_s, match_r.at[s], mate)
-
-    def compact_columns(at):
-        return remote(slim.at[1, :, at], slim_in.at[1, :, at], slim_s, slim_r.at[1], to_mid)
-
-    def hand_few(s, side):
-        at = slim_hid.at[s, side]
-        return remote(at, at, few_s, few_r.at[s], mate)
 
     named = lax.broadcasted_iota(jnp.int32, wt.shape[1:], 0)
     routes = None
@@ -208,25 +165,85 @@
         table(z, 0, to_end).start()
         table(z, 1, to_far).start()
 
+    local[0].wait()
+
+    @pl.when(outer)
+    def _():
+        for q in range(PIECES):
+            gather(z, q, 0, to_mid, own).start()
+
+    @pl.when(inner)
+    def _():
+        for q in range(LEAD):
+            gather(z, q, 1, to_far, own).start()
+
+    for q in range(PIECES):
+        swap(q).start()
+    for m in range(3):
+        local[4 + m].wait()
+        for u in range(CUTS):
+            send_y(m, u).start()
+    send_extra().start()
+    local[1].wait()
+
+    def gather_sent(b, way, dev):
+        remote(x.at[b, c], x.at[b, c], gat_s.at[way, b], gat_r.at[b, 0], dev).wait_send()
+
+    def share(b, q):
+        at = x.at[b, c, span(q)]
+        return remote(at, at, half_s.at[b], half_r.at[b, q // per_unit], mate)
+
+    def shared(b, part_of):
+        at = x.at[b, 1 - c, rows_of(part_of)]
+        remote(at, at, half_s.at[b], half_r.at[b, part_of], mate).wait_recv()
+
+    def rows_of(part_of):
+        return pl.ds(part_of * unit if isinstance(part_of, int) else pl.multiple_of(part_of * unit, unit), unit)
+
+    def thin(r):
+        size = piece // SPLIT
+        return pl.ds(r * size if isinstance(r, int) else pl.multiple_of(r * size, size), size)
+
+    def total(b, q, dev):
+        return remote(part.at[b, thin(q)], came.at[b, thin(q)], sum_s.at[b], sum_r.at[b, q], dev)
+
+    def total_sent(b, dev):
+        remote(part.at[b], came.at[b], sum_s.at[b], sum_r.at[b, 0], dev).wait_send()
+
+    def compact(s, dev):
+        return remote(slim.at[s], slim_in.at[s], slim_s, slim_r.at[s], dev)
+
+    def hand(pair, s):
+        at = hid.at[2 * pair + s, c]
+        return remote(at, at, hid_s, hid_r.at[pair], mate)
+
+    def chosen_rows(s, dev):
+        at = picked.at[s, c]
+        return remote(at, at, pick_s, pick_r.at[s], dev)
+
+    def match(s, side):
+        at = picked.at[s, side]
+        return remote(at, at, match_s, match_r.at[s], mate)
+
+    def compact_columns(at):
+        return remote(slim.at[1, :, at], slim_in.at[1, :, at], slim_s, slim_r.at[1], to_mid)
+
+    def hand_few(s, side):
+        at = slim_hid.at[s, side]
+        return remote(at, at, few_s, few_r.at[s], mate)
+
+    def normed(b, at, first, second):
+        a, d = first.astype(f32), second.astype(f32)
+        squares = jnp.sum(a * a, axis=-1, keepdims=True) + jnp.sum(d * d, axis=-1, keepdims=True)
+        scale = lax.rsqrt(squares / (2 * half) + 1e-06)
+        xn[b, 0, at] = (a * scale * gain_ref[0]).astype(bf16)
+        xn[b, 1, at] = (d * scale * gain_ref[1]).astype(bf16)
+
     def norm(q, carry):
         swap(q).wait_recv()
         at = span(q)
-        a = own[at].astype(f32)
-        b = raw[at].astype(f32)
-        total_sq = jnp.sum(a * a, axis=-1, keepdims=True) + jnp.sum(b * b, axis=-1, keepdims=True)
-        scale = lax.rsqrt(total_sq / (2 * half) + 1e-06)
-        x[z, c, at] = (a * scale * gain_ref[c]).astype(bf16)
-        x[z, 1 - c, at] = (b * scale * gain_ref[1 - c]).astype(bf16)
-
-        @pl.when(outer)
-        def _():
-            gather(z, q, 0, to_mid).start()
-
-        @pl.when(inner)
-        def _():
-            @pl.when(q < LEAD)
-            def _():
-                gather(z, q, 1, to_far).start()
+        mine, other = own[at], raw[at]
+        normed(z, at, jnp.where(c == 0, mine, other), jnp.where(c == 0, other, mine))
         return carry
 
     lax.fori_loop(0, PIECES, norm, 0)
@@ -239,13 +256,19 @@
                 for v in range(2):
                     u = n % (CUTS // 2) * 2 + v
                     send_y(m, u).wait_recv()
-                    send_x(m, u, g).start()
+
+                    @pl.when((m < 2) | (u < CUTS - 2))
+                    def _():
+                        send_x(m, u, g).start()
 
     def got_x(m):
         send_x(m, 0, 1 - g, CUTS).wait_recv()
 
     def got_columns(k):
-        send_x(2, 2 * k, 1 - g, 2).wait_recv()
+        if k == CUTS // 2 - 1:
+            send_extra().wait_recv()
+        else:
+            send_x(2, 2 * k, 1 - g, 2).wait_recv()
 
     def outer_stream(j):
         b = jnp.where(j < PIECES, far_end, far_mid)
@@ -278,7 +301,7 @@
         @pl.when(q == PIECES - 1)
         def _():
             for late in range(LEAD, PIECES):
-                gather(z, late, 1, to_far).start()
+                gather(z, late, 1, to_far, own).start()
 
     def pick(table_rows, e):
         lane = lax.broadcasted_iota(jnp.int32, table_rows.shape, 0)
@@ -312,7 +335,7 @@
 
     def pick_rows(s):
         mark, _ = selection(mid, end * COLS + (y if s == 0 else 1 - y))
-        picked[s, c] = jnp.dot(mark.astype(bf16), x[mid, c], preferred_element_type=f32).astype(bf16)
+        picked[s, c] = jnp.dot(mark.astype(bf16), xn[mid, c], preferred_element_type=f32).astype(bf16)
         chosen_rows(s, to_end).start()
 
     def got_rows(s):
@@ -338,17 +361,11 @@
     def columns_at(k, portion):
         return pl.ds(pl.multiple_of((portion * (CUTS // 2) + k) * columns_cut, columns_cut), columns_cut)
 
-    def slim_columns(k):
-        for portion in (g, 1 - g):
-            at = columns_at(k, portion)
-            got = jnp.dot(slim_hid[1, 0], wd[1, :wide, at], preferred_element_type=f32) + jnp.dot(
-                slim_hid[1, 1], wd[1, wide:, at], preferred_element_type=f32
-            )
-            slim[1, :, at] = (got * slim_w[...]).astype(bf16)
-
-    def send_columns(k):
-        for portion in (g, 1 - g):
-            compact_columns(columns_at(k, portion)).start()
+    def slim_columns(at):
+        got = jnp.dot(slim_hid[1, 0], wd[1, :wide, at], preferred_element_type=f32) + jnp.dot(
+            slim_hid[1, 1], wd[1, wide:, at], preferred_element_type=f32
+        )
+        slim[1, :, at] = (got * slim_w[...]).astype(bf16)
 
     def widen(s):
         mark, _ = selection(mid, end * COLS + (y if s == 0 else 1 - y))
@@ -365,9 +382,11 @@
         @pl.when((s == 0) & (b != z))
         def _():
             shared(b, part_of)
+            at = rows_of(part_of)
+            normed(b, at, x[b, 0, at], x[b, 1, at])
 
         at = rows_of(part_of)
-        hid[code, c] = hidden_half(x[b, 0, at], x[b, 1, at], s)
+        hid[code, c] = hidden_half(xn[b, 0, at], xn[b, 1, at], s)
         hand(pair, s).start()
 
     def second_stage(pair):
@@ -394,19 +413,23 @@
 
         @pl.when(outer & (b != z))
         def _():
-            for n in range(per_unit):
-                total(b, part_of * per_unit + n, to_mid).start()
+            for n in range(per_unit * SPLIT):
+                total(b, part_of * per_unit * SPLIT + n, to_mid).start()
 
     def pass_on(b, q, dev):
-        total(b, q, dev).wait_recv()
-        at = span(q)
-        part[b, at] = (part[b, at].astype(f32) + came[b, at].astype(f32)).astype(bf16)
-        total(b, q, dev).start()
+        for v in range(SPLIT):
+            r = q * SPLIT + v
+            total(b, r, dev).wait_recv()
+            at = thin(r)
+            part[b, at] = (part[b, at].astype(f32) + came[b, at].astype(f32)).astype(bf16)
+            total(b, r, dev).start()
 
     def take_in(q):
-        total(z, q, to_far).wait_recv()
-        at = span(q)
-        acc[at] = acc[at] + came[z, at].astype(f32)
+        for v in range(SPLIT):
+            r = q * SPLIT + v
+            total(z, r, to_far).wait_recv()
+            at = thin(r)
+            acc[at] = acc[at] + came[z, at].astype(f32)
 
     def look(n, entries):
         value = 0
@@ -452,9 +475,6 @@
         packed(outer_second, second_width), packed(inner_second, second_width),
     )
 
-    for copy in local[4:]:
-        copy.wait()
-
     @pl.when(outer)
     def _():
         table(mid, 0, to_mid).wait_recv()
@@ -528,16 +548,22 @@
             for k in range(CUTS // 2):
                 @pl.when(n == min(head, PIECES + 2 + k))
                 def _():
-                    got_columns(k)
                     if k == 0:
                         hand_few(1, 1 - c).wait_recv()
-                    if k < CUTS // 2 - 1:
-                        slim_columns(k)
-                        send_columns(k)
+                    for early in ((0, 1), (2,), (), ())[k]:
+                        at = columns_at(early, g)
+                        slim_columns(at)
+                        compact_columns(at).start()
+                    got_columns(k)
+                    if k < 2:
+                        at = columns_at(k, 1 - g)
+                        slim_columns(at)
+                        compact_columns(at).start()
 
             @pl.when(n == head + 2)
             def _():
-                slim_columns(CUTS // 2 - 1)
+                for k, portion in ((3, g), (2, 1 - g), (3, 1 - g)):
+                    slim_columns(columns_at(k, portion))
 
         @pl.when(outer)
         def _():
@@ -609,26 +635,31 @@
 
         @pl.when(outer & (n == 3 * PIECES + 2))
         def _():
-            send_columns(CUTS // 2 - 1)
+            for k, portion in ((3, g), (2, 1 - g), (3, 1 - g)):
+                compact_columns(columns_at(k, portion)).start()
         return carry
 
     lax.fori_loop(0, 4 * PIECES, step, 0)
 
     @pl.when(outer)
     def _():
-        for q in range(PIECES):
-            total(z, q, to_mid).wait_recv()
-            at = span(q)
+        def close(r, carry):
+            total(z, r, to_mid).wait_recv()
+            at = thin(r)
             out_ref[at] = (acc[at] + came[z, at].astype(f32)).astype(bf16)
+            return carry
+
+        lax.fori_loop(0, PIECES * SPLIT, close, 0)
 
     @pl.when(inner)
     def _():
         out_ref[...] = acc[...].astype(bf16)
 
     swap(0, PIECES).wait_send()
+    send_extra().wait_send()
     for m in range(3):
         send_y(m, 0, CUTS).wait_send()
-        send_x(m, 0, g, CUTS).wait_send()
+        send_x(m, 0, g, CUTS if m < 2 else CUTS - 2).wait_send()
 
     def handed(count):
         at = hid.at[pl.ds(0, count), c]
@@ -686,8 +717,8 @@
     bits = (length, PIECES)
     sems = [dma, dma((PIECES,)), dma((7,))]
     for send, recv in (
-        ((3,), (3, CUTS)), ((3,), (2 + CUTS // 2,)), ((2, length), bits), ((2, length), (length,)),
-        ((length,), (length, UNITS)), ((), (pairs,)), ((), (2,)), ((), (2,)), ((), (2,)), ((length,), bits), ((), (2,)),
+        ((4,), (3, CUTS)), ((3,), (2 + CUTS // 2,)), ((2, length), bits), ((2, length), (length,)),
+        ((length,), (length, UNITS)), ((), (pairs,)), ((), (2,)), ((), (2,)), ((), (2,)), ((length,), (length, PIECES * SPLIT)), ((), (2,)),
     ):
         sems += [dma(send) if send else dma, dma(recv)]
     return pl.pallas_call(
@@ -701,6 +732,7 @@
             vmem((top, tok_rows), jnp.int32),
             vmem((top, tok_rows), f32),
             vmem((tok_rows, half), bf16),
+            vmem((length, 2, tok_rows, half), bf16),
             vmem((length, 2, tok_rows, half), bf16),
             vmem((length, experts, tok_rows), f32),
             vmem((length, tok_rows, experts), f32),

time: 99.6 us -> 97.7 us (0.981)
  Pallas kernels: 98.5 us -> 96.5 us
    pallas_call x1, Pallas kernels: 98.5 us -> 96.5 us  [line_form(): pl.pallas_call(functools.partial(line_kernel, length, cap), out_shape=vme...]
where the time goes in v4:
time: 97.7 us; the launch traced here: 97.5 us
  Pallas kernels  96.5 us (99%)
    pallas_call x1, Pallas kernels, line_form(): pl.pallas_call(functools.partial(line_kernel, length, cap), out_shape=vme...  96.5 us

profile of v4, /device:TPU:8, one launch (start us, length us, event | category | flops | bytes accessed | tf_op | source)
XLA Modules:
  0.0 97.5 jit_solution(14046356865417753797)
XLA Ops:
  0.0 96.5 %shard_map.73 = bf16[512,1024]{1,0:T(8,128)(2,1)S(1)} custom-call(bf16[512,1024]{1,0:T(8,128)(2,1)} %tok_ref.1, f32[2,1,1024]{2,1,0:T(1,128)} %bitcast.9, s32[2,512]{1,0:T(2,128)} %bitcast.10, f32[2,512]{1,0:T(2,128)} %bitcast.11, bf16[2048,256]{1,0:T(8,128)(2,1)} %bitcast.6, bf16[2048,256]{1,0:T(8,128)(2,1)} %bitcast.7, bf16[512,1024]{1,0:T(8,128)(2,1)} %bitcast.8), custom_call_target="tpu_custom_call" | custom-call | tf_op jit(solution)/shard_map/pallas_call | solution.py:724
  96.5 1.0 copy.9

commit v5 on v4

--- a/solution.py
+++ b/solution.py
@@ -439,15 +439,15 @@
 
     head = 3 * CUTS // 2
     outer_first = {
-        0: ((1, 0, 0), (1, 1, 0)), 1: ((1, 2, 0), (1, 3, 0)), 10: ((0, 0, 0), (0, 0, 1)), 11: ((0, 1, 0), (0, 1, 1)),
-        13: ((0, 2, 0), (0, 2, 1)), 14: ((1, 0, 1), (1, 1, 1)), 15: ((0, 3, 0), (0, 3, 1)), 16: ((1, 2, 1), (1, 3, 1)),
+        0: ((1, 0, 0), (1, 1, 0)), 1: ((1, 2, 0), (1, 3, 0)), 10: ((0, 0, 0), (0, 0, 1)), 13: ((0, 1, 0), (0, 1, 1)),
+        14: ((0, 2, 0), (0, 2, 1)), 15: ((1, 0, 1), (1, 1, 1)), 16: ((0, 3, 0), (0, 3, 1)), 17: ((1, 2, 1), (1, 3, 1)),
         19: ((2, 0, 0), (2, 0, 1)), 21: ((2, 1, 0), (2, 1, 1)), 23: ((2, 2, 0), (2, 2, 1)), 25: ((2, 3, 0), (2, 3, 1)),
     }
     outer_second = {
-        12: ((0, 0), (0, 1)), 13: ((0, 2),), 15: ((0, 3),), 16: ((1, 0), (1, 1)), 17: ((1, 2), (1, 3)),
+        12: ((0, 0),), 13: ((0, 1),), 14: ((0, 2),), 16: ((0, 3),), 17: ((1, 0), (1, 1)), 18: ((1, 2), (1, 3)),
         19: ((2, 0),), 21: ((2, 1),), 23: ((2, 2),), 25: ((2, 3),),
     }
-    outer_pairs = {13: 5, 15: 7, 18: 9, 20: 11, 22: 13, 24: 15}
+    outer_pairs = {14: 5, 16: 7, 18: 9, 20: 11, 22: 13, 24: 15}
     inner_first = {
         0: ((3, 0, 0), (3, 1, 0)), 1: ((3, 2, 0), (3, 3, 0)), 2: ((1, 0, 0),), 3: ((2, 0, 0),),
         4: ((1, 1, 0), (0, 0, 0)), 6: ((1, 2, 0), (0, 1, 0)), 8: ((1, 3, 0), (0, 2, 0)),
@@ -491,6 +491,10 @@
             columns[b] = wt[b].T
 
     def step(n, carry):
+        @pl.when(inner & (n < PIECES))
+        def _():
+            inner_end(n)
+
         @pl.when(n < head)
         def _():
             got_y(n)
@@ -520,10 +524,6 @@
 
         @pl.when(inner)
         def _():
-            @pl.when(n < PIECES)
-            def _():
-                inner_end(n)
-
             @pl.when((n < head) | ((n >= head + 2) & (n < head + 6)))
             def _():
                 inner_stream(jnp.where(n < head, n, n - 2))
@@ -560,7 +560,7 @@
                         slim_columns(at)
                         compact_columns(at).start()
 
-            @pl.when(n == head + 2)
+            @pl.when(n == head + 3)
             def _():
                 for k, portion in ((3, g), (2, 1 - g), (3, 1 - g)):
                     slim_columns(columns_at(k, portion))
@@ -599,6 +599,8 @@
             def _():
                 compact(1, to_end).wait_recv()
                 acc[...] = acc[...] + widen(1)
+                early = pl.ds(0, rows - piece)
+                out_ref[early] = acc[early].astype(bf16)
 
             @pl.when(q >= PIECES + 2)
             def _():
@@ -653,7 +655,8 @@
 
     @pl.when(inner)
     def _():
-        out_ref[...] = acc[...].astype(bf16)
+        end_rows = pl.ds(rows - piece, piece)
+        out_ref[end_rows] = acc[end_rows].astype(bf16)
 
     swap(0, PIECES).wait_send()
     send_extra().wait_send()

time: 97.7 us -> 97.5 us (level)
  no operation moved by 1% of the time
where the time goes in v5:
time: 97.5 us; the launch traced here: 97.4 us
  Pallas kernels  96.4 us (99%)
    pallas_call x1, Pallas kernels, line_form(): pl.pallas_call(functools.partial(line_kernel, length, cap), out_shape=vme...  96.4 us

profile of v5, /device:TPU:8, one launch (start us, length us, event | category | flops | bytes accessed | tf_op | source)
XLA Modules:
  0.0 97.4 jit_solution(2704170259918389931)
XLA Ops:
  0.0 96.4 %shard_map.73 = bf16[512,1024]{1,0:T(8,128)(2,1)S(1)} custom-call(bf16[512,1024]{1,0:T(8,128)(2,1)} %tok_ref.1, f32[2,1,1024]{2,1,0:T(1,128)} %bitcast.9, s32[2,512]{1,0:T(2,128)} %bitcast.10, f32[2,512]{1,0:T(2,128)} %bitcast.11, bf16[2048,256]{1,0:T(8,128)(2,1)} %bitcast.6, bf16[2048,256]{1,0:T(8,128)(2,1)} %bitcast.7, bf16[512,1024]{1,0:T(8,128)(2,1)} %bitcast.8), custom_call_target="tpu_custom_call" | custom-call | tf_op jit(solution)/shard_map/pallas_call | solution.py:727
  96.4 1.0 copy.9
